TPU v7x, 32 devices: a whole 2x2x4 slice. The times are simulated.
32 devices in a mesh: grp: 2 (over y), kv: 4 (over z), tp: 4 (over x, core).
Axes of the slice: x: 2, y: 2, z: 4, core: 2. Of those that a mesh axis runs over, the one named last changes fastest.
Arguments:
- candidate_embeddings: bfloat16 [1536, 4096], P(('grp', 'kv'), 'tp'), parts along dimension 0, may hold values from -100 to 100
- incoming_rms_scaling: float32 [4096], replicated, may hold values from 0.1 to 1.9
- probe_projector: bfloat16 [4096, 2048], P('kv', 'tp'), may hold values from -0.09375 to 0.09375
- address_projector: bfloat16 [4096, 2048], P('kv', 'tp'), may hold values from -0.09375 to 0.09375
- content_projector: bfloat16 [4096, 2048], P('kv', 'tp'), may hold values from -0.09375 to 0.09375
- sigmoid_mask_matrix: bfloat16 [4096, 2048], P('kv', 'tp'), may hold values from -0.09375 to 0.09375
- forgetting_projector: bfloat16 [4096, 16], replicated, may hold values from -0.09375 to 0.09375
- strength_projector_matrix: bfloat16 [4096, 16], replicated, may hold values from -0.09375 to 0.09375
- channel_forgetting_rates: float32 [16], P('tp'), may hold values from -3 to 0.5
- forgetting_offset: float32 [16], P('tp'), may hold values from -1 to 1
- extra_forgetting: float32 [384, 4, 16], P(('grp', 'kv'), None, 'tp'), parts along dimension 0, may hold values from -0.7 to 0, as said below
- outgoing_rms_scaling: float32 [128], replicated, may hold values from 0.1 to 1.9
- final_projector: bfloat16 [2048, 4096], P('tp', 'kv'), may hold values from -0.125 to 0.125
- memory_matrix: float32 [384, 16, 128, 128], P(('grp', 'kv'), 'tp'), parts along dimension 0, may hold values from -4 to 4
- earlier_addresses: bfloat16 [384, 4, 16, 128], P(('grp', 'kv'), None, 'tp'), parts along dimension 0, may hold values from -6 to 6
- earlier_contents: bfloat16 [384, 4, 16, 128], P(('grp', 'kv'), None, 'tp'), parts along dimension 0, may hold values from -6 to 6
- earlier_strengths: float32 [384, 4, 16], P(('grp', 'kv'), None, 'tp'), parts along dimension 0, may hold values from 0.1 to 0.9
- earlier_forgetting: float32 [384, 4, 16], P(('grp', 'kv'), None, 'tp'), parts along dimension 0, may hold values from -1.5 to -0.02
- admitted_counts: int32 [384], P(('grp', 'kv')), parts along dimension 0, may hold values from 0 to 4
Outputs:
- mixed: bfloat16 [1536, 4096], P(('grp', 'kv'), 'tp'), parts along dimension 0
- taken_state: float32 [384, 16, 128, 128], P(('grp', 'kv'), 'tp'), parts along dimension 0
There are 2 independent parts, one for each index of `grp`. A program takes and returns all parts, laid end to end along the dimension named above; an argument that names none is the same for every part. Nothing has to cross between parts.
Inputs may be any that keep to these rules, and one draw needn't show every extreme that they name: `extra_forgetting`: mostly zero; elsewhere the logarithm of a factor between 0.5 and 0.8.
All inputs are finite; a program needn't handle non-finite values.
Results may differ from a plain program's by a relative error of at most 0.015.
Values may be sent and summed in bfloat16 or wider, within the bound.
No kernel may reach another device: no remote copies, remote signals or barrier semaphores. Data moves between devices by JAX's collectives and lax.ppermute only.
A program may use at most 128 MiB of HBM per device.

v0:
```python
import functools

import jax
import jax.numpy as jnp
from jax import lax
from jax.experimental import pallas as pl
from jax.experimental.pallas import tpu as pltpu
from jax.sharding import PartitionSpec as P


DK = 128
P_SIZE = 4
CORES = 2
CHUNKS = 1
PIECES = 3
ENDS = 2
VMEM_LIMIT = 50 * 2**20
BLOCK = 8

epsilon = 1e-06
f32 = jnp.float32
bf16 = jnp.bfloat16


def rows_of(outs, index):
    row = lax.broadcasted_iota(jnp.int32, (BLOCK, DK), 0)
    result = outs[0][index * BLOCK : (index + 1) * BLOCK]
    for s in range(1, BLOCK):
        result = jnp.where(row == s, outs[s][index * BLOCK : (index + 1) * BLOCK], result)
    return result


def split_two(values):
    high = values.astype(bf16)
    low = (values - high.astype(f32)).astype(bf16)
    return high, low


def state_products(vectors, state_ref, h):
    left = jnp.concatenate(vectors, axis=0).astype(bf16)
    if state_ref.dtype == f32:
        left = jnp.concatenate([left, left], axis=1)
    outs = []
    for p in range(BLOCK // 2):
        both = jnp.concatenate([state_ref[2 * p, h], state_ref[2 * p + 1, h]], axis=1)
        if state_ref.dtype == f32:
            both = jnp.concatenate(split_two(both), axis=0)
        out = jnp.dot(left, both, preferred_element_type=f32)
        outs += [out[:, :DK], out[:, DK:]]
    return outs


def row_dot(a, b):
    return jnp.sum(a * b, axis=1, keepdims=True)


def decay_tables(log_decays):
    total = log_decays[0]
    starts = [jnp.exp(total)]
    for t in range(1, P_SIZE):
        total = total + log_decays[t]
        starts.append(jnp.exp(total))
    between = {}
    for i in range(P_SIZE):
        total = None
        for t in range(i + 1, P_SIZE):
            total = log_decays[t] if total is None else total + log_decays[t]
            between[i, t] = jnp.exp(total)
    return starts, between


def take_kernel(start, last_ref, aux_ref, key_ref, value_ref, state_ref, *refs):
    out_ref, rounded_ref = refs[-2:]
    heads = state_ref.shape[1]
    base = (start + pl.program_id(0)) * BLOCK
    aux = [aux_ref[pl.ds(j, BLOCK, stride=P_SIZE), :] for j in range(P_SIZE)]
    starts, between = decay_tables(aux)
    row_index = lax.broadcasted_iota(jnp.int32, (2 * P_SIZE * BLOCK, DK), 0) % BLOCK
    for h in range(heads):
        col = lambda table, lane=h: table[:, lane : lane + 1]
        keys = [key_ref[j, h] for j in range(P_SIZE)]
        outs = state_products(keys, state_ref, h)
        norms = [lax.rsqrt(row_dot(k, k) + epsilon) for k in keys]
        writes = []
        for j in range(P_SIZE):
            value = value_ref[j, h] - (col(starts[j]) * norms[j]) * rows_of(outs, j)
            for i in range(j):
                factor = col(between[i, j]) * norms[i] * norms[j] * row_dot(keys[i], keys[j])
                value = value - factor * writes[i]
            writes.append(col(aux[j], heads + h) * value)
        ends = []
        for j in range(P_SIZE):
            factor = norms[j] if j == P_SIZE - 1 else norms[j] * col(between[j, P_SIZE - 1])
            ends.append(factor * writes[j])
        ends = jnp.concatenate(ends, axis=0)
        high = ends.astype(bf16).astype(f32)
        ends = jnp.concatenate([high, ends - high], axis=0)
        left = jnp.concatenate(keys + keys, axis=0).astype(bf16)
        for p in range(BLOCK // 2):
            masked = jnp.concatenate(
                [jnp.where(row_index == 2 * p + e, ends, 0.0) for e in range(2)], axis=1
            ).astype(bf16)
            added = lax.dot_general(
                left, masked, (((0,), (0,)), ((), ())), preferred_element_type=f32
            )
            for e in range(2):
                s = 2 * p + e
                taken = last_ref[base + s, h] * state_ref[s, h] + added[:, e * DK : (e + 1) * DK]
                out_ref[s, h] = taken
                rounded_ref[s, h] = taken.astype(bf16)


def take(piece, before, memory, keys, values, aux, last):
    seqs, heads = memory.shape[:2]
    steps = seqs // BLOCK // PIECES
    start = piece * steps
    vector_spec = pl.BlockSpec((P_SIZE, heads, BLOCK, DK), lambda i: (0, 0, start + i, 0))
    state_spec = pl.BlockSpec((BLOCK, heads, DK, DK), lambda i: (start + i, 0, 0, 0))
    in_specs = [
        pl.BlockSpec(memory_space=pltpu.SMEM),
        pl.BlockSpec((BLOCK * P_SIZE, 128), lambda i: (start + i, 0)),
        vector_spec,
        vector_spec,
        state_spec,
    ]
    operands = [last, aux, keys, values, memory]
    aliases = {}
    if before is not None:
        in_specs += [pl.BlockSpec(memory_space=pl.ANY)] * 2
        aliases = {len(operands): 0, len(operands) + 1: 1}
        operands += before
    return pl.pallas_call(
        functools.partial(take_kernel, start),
        grid=(steps,),
        in_specs=in_specs,
        out_specs=[state_spec, state_spec],
        out_shape=[jax.ShapeDtypeStruct(memory.shape, kind) for kind in (f32, bf16)],
        input_output_aliases=aliases,
        compiler_params=pltpu.CompilerParams(vmem_limit_bytes=VMEM_LIMIT),
        cost_estimate=pl.CostEstimate(
            flops=memory.size * 64 // PIECES,
            bytes_accessed=memory.size * 8 // PIECES,
            transcendentals=0,
        ),
        name="take",
    )(*operands)


def finish_kernel(n_refs, position_ref, aux_ref, gain_ref, own_ref, right_ref, left_ref, *refs):
    state_ref, *refs = refs
    near_refs, far_refs, refs = refs[:n_refs], refs[n_refs : 2 * n_refs], refs[2 * n_refs :]
    away_ref, home_ref, acc, vectors, found_ref, flat, weights, sems = refs
    heads = state_ref.shape[1]
    step = pl.program_id(0)
    seqs = vectors.shape[2]
    rows = BLOCK * P_SIZE
    n_blocks = weights.shape[0]

    def each_copy(act):
        for k in range(n_refs):

            @pl.when(position_ref[k] >= 0)
            def _():
                for side, refs in enumerate((near_refs, far_refs)):
                    into = weights.at[position_ref[k], side]
                    act(pltpu.make_async_copy(refs[k], into, sems.at[k, side]))

    @pl.when(step == 0)
    def _():
        each_copy(lambda copy: copy.start())

    scale = aux_ref[pl.ds(step * rows, rows), :][:, 2 * heads : 2 * heads + 1]
    here = pl.ds(step * BLOCK, BLOCK)
    for kind in range(4):
        for h in range(heads):
            at = pl.ds((kind * heads + h) * DK, DK)
            total = own_ref[:, at] + right_ref[:, at].astype(f32) + left_ref[:, at].astype(f32)
            acc[kind * heads + h] = (total * scale).astype(bf16).astype(f32)
    for h in range(heads):
        picked = [
            acc[kind * heads + h, pl.ds(t, BLOCK, stride=P_SIZE), :]
            for kind in range(4)
            for t in range(P_SIZE)
        ]
        for n, value in enumerate(picked):
            vectors[n, h, here, :] = value
        outs = state_products(picked[: 2 * P_SIZE], state_ref, h)
        for n in range(2 * P_SIZE):
            found_ref[n, h, here, :] = rows_of(outs, n)

    @pl.when(step == pl.num_programs(0) - 1)
    def _():
        def whole(ref, n):
            return ref[n].reshape(heads * seqs, DK)

        def spread(table, first=0):
            return jnp.concatenate(
                [
                    jnp.broadcast_to(table[:, first + h : first + h + 1], (seqs, DK))
                    for h in range(heads)
                ],
                axis=0,
            )

        aux = [aux_ref[pl.ds(t, seqs, stride=P_SIZE), :] for t in range(P_SIZE)]
        starts, between = decay_tables(aux)
        gain = gain_ref[...]
        queries = [whole(vectors, t) for t in range(P_SIZE)]
        keys = [whole(vectors, P_SIZE + t) for t in range(P_SIZE)]
        norms = [lax.rsqrt(row_dot(k, k) + epsilon) for k in keys]
        writes = []
        for t in range(P_SIZE):
            start = spread(starts[t])
            steps = {i: spread(between[i, t]) for i in range(t)}
            value = whole(vectors, 2 * P_SIZE + t) - start * norms[t] * whole(found_ref, P_SIZE + t)
            for i in range(t):
                factor = steps[i] * (norms[i] * norms[t] * row_dot(keys[i], keys[t]))
                value = value - factor * writes[i]
            writes.append(spread(aux[t], heads) * value)
            query = queries[t]
            found = start * whole(found_ref, t)
            for i in range(t + 1):
                factor = norms[i] * row_dot(keys[i], query)
                if i < t:
                    factor = factor * steps[i]
                found = found + factor * writes[i]
            attended = found * (lax.rsqrt(row_dot(query, query) + epsilon) * DK ** (-0.5))
            mean = jnp.mean(attended * attended, axis=1, keepdims=True)
            gate = whole(vectors, 3 * P_SIZE + t)
            scaled = attended * lax.rsqrt(mean + epsilon) * gain * (gate * jax.nn.sigmoid(gate))
            for h in range(heads):
                flat[h, pl.ds(t, seqs, stride=P_SIZE), :] = scaled[h * seqs : (h + 1) * seqs]
        sides = heads // 2
        plane = position_ref[n_refs]
        lefts = [
            jnp.concatenate([flat[first + h] for h in range(sides)], axis=1).astype(bf16)
            for first in (plane * sides, (1 - plane) * sides)
        ]
        each_copy(lambda copy: copy.wait())
        cols = weights.shape[-1]
        for n in range(n_blocks):
            result = sum(
                jnp.dot(lefts[side], weights[n, side], preferred_element_type=f32)
                for side in range(2)
            ).astype(bf16)
            out_ref, at = (away_ref, n) if n < n_blocks // 2 else (home_ref, n - n_blocks // 2)
            out_ref[:, pl.ds(at * cols, cols)] = result


def finish(chunk, n_blocks, own, right, left, state, aux, gain, near, far, position):
    seqs, heads = state.shape[:2]
    rows = BLOCK * P_SIZE
    steps = seqs // BLOCK // ENDS
    start = chunk * steps
    first = start % (own.shape[0] // rows)
    n_refs = len(near)
    half, cols = near[0].shape
    part_spec = lambda at: pl.BlockSpec((rows, 4 * heads * DK), lambda i: (at + i, 0))
    out = jax.ShapeDtypeStruct((steps * rows, n_blocks // 2 * cols), bf16)
    out_spec = pl.BlockSpec(out.shape, lambda i: (0, 0))
    return pl.pallas_call(
        functools.partial(finish_kernel, n_refs),
        grid=(steps,),
        in_specs=[
            pl.BlockSpec(memory_space=pltpu.SMEM),
            pl.BlockSpec((steps * rows, 128), lambda i: (chunk, 0)),
            pl.BlockSpec((1, DK), lambda i: (0, 0)),
            part_spec(first),
            part_spec(0),
            part_spec(0),
            pl.BlockSpec((BLOCK, heads, DK, DK), lambda i: (start + i, 0, 0, 0)),
            *[pl.BlockSpec(memory_space=pl.ANY)] * (2 * n_refs),
        ],
        out_specs=[out_spec, out_spec],
        out_shape=[out, out],
        scratch_shapes=[
            pltpu.VMEM((4 * heads, rows, DK), f32),
            pltpu.VMEM((4 * P_SIZE, heads, steps * BLOCK, DK), f32),
            pltpu.VMEM((2 * P_SIZE, heads, steps * BLOCK, DK), f32),
            pltpu.VMEM((heads, steps * rows, DK), f32),
            pltpu.VMEM((n_blocks, 2, half, cols), bf16),
            pltpu.SemaphoreType.DMA((n_refs, 2)),
        ],
        compiler_params=pltpu.CompilerParams(vmem_limit_bytes=VMEM_LIMIT),
        cost_estimate=pl.CostEstimate(
            flops=state.size * 64 // ENDS,
            bytes_accessed=state.size * 2 // ENDS,
            transcendentals=0,
        ),
        name="finish",
    )(position, aux, gain, own, right, left, state, *near, *far)


def after(value, *others):
    return lax.optimization_barrier((value, *others))[0]


def on_device(
    sizes,
    candidate_embeddings,
    incoming_rms_scaling,
    probe_projector,
    address_projector,
    content_projector,
    sigmoid_mask_matrix,
    forgetting_projector,
    strength_projector_matrix,
    channel_forgetting_rates,
    forgetting_offset,
    extra_forgetting,
    outgoing_rms_scaling,
    final_projector,
    memory_matrix,
    earlier_addresses,
    earlier_contents,
    earlier_strengths,
    earlier_forgetting,
    admitted_counts,
):
    _, n_kv, n_tp = sizes
    rows, local_cols = candidate_embeddings.shape
    width = probe_projector.shape[1]
    heads = width // DK
    all_heads = forgetting_projector.shape[1]
    model = local_cols * n_tp
    per_tp = n_kv // n_tp
    kv_cols = model // n_kv
    z = lax.axis_index("kv")
    tp = lax.axis_index("tp")
    plane = lax.axis_index("grp")
    core = tp % CORES

    def swap(value, mask):
        return lax.ppermute(value, "tp", [(i, i ^ mask) for i in range(n_tp)])

    chunk_rows = rows // CHUNKS
    part_rows = chunk_rows // CORES

    gain_part = lax.dynamic_slice_in_dim(incoming_rms_scaling, tp * local_cols, local_cols)
    gained = (candidate_embeddings.astype(f32) * gain_part).astype(bf16)
    halves = []
    for chunk in range(CHUNKS):
        pieces = []
        for m in range(n_tp):
            at = chunk * chunk_rows + part_rows * ((tp ^ m) % CORES)
            pieces.append(lax.dynamic_slice_in_dim(gained, at, part_rows))
        for m in range(n_tp - 1, 0, -1):
            pieces[m] = swap(pieces[m], m)
        halves.append(jnp.stack(pieces))

    half = width // 2
    near = lax.dynamic_slice_in_dim(final_projector, plane * half, half)
    far = lax.dynamic_slice_in_dim(final_projector, (1 - plane) * half, half)
    rights, lefts = [near], [near]
    far_rights, far_lefts = [far], [far]

    def weight_round(i, *others):
        right, left = lax.optimization_barrier((rights[-1], lefts[-1], *others))[:2]
        pairs = [(j, j + 1) for j in range(i - 1, n_kv - 1)]
        rights.append(lax.ppermute(right, "kv", pairs))
        pairs = [(j + 1, j) for j in range(0, n_kv - i)]
        lefts.append(lax.ppermute(left, "kv", pairs))

    def weight_cross(i):
        def pairs(places):
            return [(g * n_kv + j, (1 - g) * n_kv + j) for g in range(2) for j in places]

        both = ("grp", "kv")
        right, left = lax.optimization_barrier((rights[i], lefts[i]))
        far_rights.append(lax.ppermute(right, both, pairs(range(i, n_kv))))
        far_lefts.append(lax.ppermute(left, both, pairs(range(n_kv - i))))

    weight_round(1, gained)

    joined = jnp.concatenate(
        [probe_projector, address_projector, content_projector, sigmoid_mask_matrix], axis=1
    )

    received = []
    for chunk in range(CHUNKS):

        def block_for(dest):
            return lax.dynamic_slice(
                halves[chunk],
                (tp ^ (dest // per_tp), 0, (dest % per_tp) * kv_cols),
                (1, part_rows, kv_cols),
            )[0]

        sends = lax.optimization_barrier(tuple(block_for((z + k) % n_kv) for k in range(n_kv)))
        received.append(
            [sends[0]]
            + [
                lax.ppermute(sends[k], "kv", [(i, (i + k) % n_kv) for i in range(n_kv)])
                for k in range(1, n_kv)
            ]
        )

    blocks = [None] * CHUNKS
    products = [{} for _ in range(CHUNKS)]
    arrived = [None] * CHUNKS
    token = received[0][0]
    crossing = crossing_order(n_kv)
    for i in range(1, n_kv):
        for chunk in range(CHUNKS):
            product = products[chunk]
            if i == 1:
                mine = lax.optimization_barrier((*received[chunk], token))[:n_kv]
                blocks[chunk] = [None] * n_kv
                for k in crossing:
                    partner = swap(mine[k], 1)
                    blocks[chunk][k] = jnp.concatenate(
                        [
                            jnp.where(core == 0, mine[k], partner),
                            jnp.where(core == 0, partner, mine[k]),
                        ]
                    )
            if i <= n_kv // 2:
                pair = [i, n_kv - i] if i < n_kv - i else [0, i]
                block = jnp.concatenate([blocks[chunk][k] for k in pair], axis=0)
                block = after(block, token)
                out = jnp.dot(block, joined, preferred_element_type=f32)
                out = lax.optimization_barrier(out)
                for n, k in enumerate(pair):
                    product[k] = out[n * chunk_rows : (n + 1) * chunk_rows]
            sends = [product[i], product[n_kv - i]]
            places = (
                [(j, j + 1) for j in range(i)],
                [(j, j - 1) for j in range(n_kv - i, n_kv)],
            )
            parts = ENDS // CHUNKS if i == n_kv - 1 else 1
            part = chunk_rows // parts
            for side in range(2):
                if arrived[chunk] is not None:
                    there = after(arrived[chunk][0][side], token)
                    sends[side] = sends[side] + there.astype(f32)
                token = sends[side] = lax.optimization_barrier(sends[side].astype(bf16))
            got = []
            for n in range(parts):
                both = []
                for side in range(2):
                    send = sends[side]
                    if parts > 1:
                        send = lax.optimization_barrier(send[n * part : (n + 1) * part])
                    both.append(lax.ppermute(send, "kv", places[side]))
                got.append(tuple(both))
            arrived[chunk] = got
            if chunk == 0:
                if 2 * i < n_kv:
                    weight_round(2 * i, token)
                for q in range(max(2 * i - 2, 1), min(2 * i, n_kv)):
                    weight_cross(q)
                if 2 * i + 1 < n_kv:
                    weight_round(2 * i + 1, token)
        if i == 1:
            first_arrived = arrived[0][0][0]

    early = lax.optimization_barrier(
        (
            admitted_counts,
            earlier_forgetting,
            earlier_strengths,
            earlier_addresses,
            earlier_contents,
            gained,
        )
    )
    live = early[0][:, None, None] > jnp.arange(P_SIZE)[None, :, None]
    early_decay = jnp.where(live, early[1], 0.0)
    early_aux = jnp.concatenate([early_decay, jnp.where(live, early[2], 0.0)], axis=2)
    early_aux = jnp.pad(early_aux.reshape(rows, 2 * heads), ((0, 0), (0, 128 - 2 * heads)))
    by_head = lambda values: jnp.transpose(values, (1, 2, 0, 3)).astype(f32)
    early_keys, early_values = by_head(early[3]), by_head(early[4])
    early_last = jnp.exp(jnp.sum(early_decay, axis=1))
    taken = None
    for piece in range(PIECES):
        taken = take(piece, taken, memory_matrix, early_keys, early_values, early_aux, early_last)

    small = jnp.concatenate([forgetting_projector, strength_projector_matrix], axis=1)
    small = lax.dynamic_slice_in_dim(small, tp * local_cols, local_cols)
    tied, raw = lax.optimization_barrier((gained, candidate_embeddings, first_arrived))[:2]
    raw = raw.astype(f32)
    sums = jnp.concatenate(
        [
            jnp.dot(tied, small, preferred_element_type=f32),
            jnp.sum(raw * raw, axis=1, keepdims=True),
        ],
        axis=1,
    )
    mask = 1
    while mask < n_tp:
        sums = sums + lax.ppermute(sums, "tp", [(i, i ^ mask) for i in range(n_tp)])
        mask *= 2
    scale = lax.rsqrt(sums[:, 2 * all_heads :] / model + epsilon)
    own = lambda at: lax.dynamic_slice_in_dim(sums, at + tp * heads, heads, 1) * scale
    log_decay = -jnp.exp(channel_forgetting_rates) * jax.nn.softplus(
        own(0) + forgetting_offset
    ) + extra_forgetting.reshape(rows, heads)
    aux = jnp.concatenate([log_decay, jax.nn.sigmoid(own(all_heads)), scale], axis=1)
    aux = jnp.pad(aux, ((0, 0), (0, 128 - aux.shape[1])))
    gain = outgoing_rms_scaling[None]

    offsets = [0] + [-i for i in range(1, n_kv)] + list(range(1, n_kv))
    source = z + jnp.array(offsets, dtype=jnp.int32)
    apart = tp ^ (source // per_tp)
    position = (apart // 2 + jnp.where(apart % 2 == 0, n_tp // 2, 0)) * per_tp + source % per_tp
    position = jnp.where((source >= 0) & (source < n_kv), position, -1)
    position = jnp.concatenate([position, plane[None]]).astype(jnp.int32)
    results = []
    for end in range(ENDS):
        chunk = end * CHUNKS // ENDS
        away, home = finish(
            end,
            n_kv,
            products[chunk][0],
            *arrived[chunk][end % (ENDS // CHUNKS)],
            taken[1],
            aux,
            gain,
            rights + lefts[1:],
            far_rights + far_lefts[1:],
            position,
        )
        home = home.astype(f32) + swap(away, 1).astype(f32)
        result = home[:, :local_cols]
        for m in range(1, n_tp // 2):
            piece = home[:, m * local_cols : (m + 1) * local_cols].astype(bf16)
            result = result + swap(piece, 2 * m).astype(f32)
        results.append(result.astype(bf16))
    return (jnp.concatenate(results, axis=0), taken[0])


def crossing_order(n_kv):
    first = [k for i in range(1, (n_kv + 1) // 2) for k in (i, n_kv - i)]
    return first + [k for k in range(n_kv) if k not in first]


def solution(mesh):
    in_specs = (
        P(("grp", "kv"), "tp"),
        P(),
        P("kv", "tp"),
        P("kv", "tp"),
        P("kv", "tp"),
        P("kv", "tp"),
        P(),
        P(),
        P("tp"),
        P("tp"),
        P(("grp", "kv"), None, "tp"),
        P(),
        P("tp", "kv"),
        P(("grp", "kv"), "tp", None, None),
        P(("grp", "kv"), None, "tp", None),
        P(("grp", "kv"), None, "tp", None),
        P(("grp", "kv"), None, "tp"),
        P(("grp", "kv"), None, "tp"),
        P(("grp", "kv")),
    )
    out_specs = (P(("grp", "kv"), "tp"), P(("grp", "kv"), "tp", None, None))
    sizes = tuple(mesh.shape[name] for name in ("grp", "kv", "tp"))

    def layer(*arrays):
        return on_device(sizes, *arrays)

    return jax.shard_map(
        layer, mesh=mesh, in_specs=in_specs, out_specs=out_specs, check_vma=False
    )
```

profile of v0, /device:TPU:0, one launch (start us, length us, event | category | flops | bytes accessed | tf_op | source)
XLA Modules:
  0.0 175.9 jit_solution(15059534556905438709)
XLA Ops:
  0.7 0.8 dynamic_slice.46
  1.5 1.1 multiply_convert_fusion
  2.6 0.9 dynamic-slice_bitcast_fusion.4
  3.5 2.4 %collective-permute-start.2 = (bf16[96,1024]{1,0:T(8,128)(2,1)}, bf16[96,1024]{1,0:T(8,128)(2,1)}, u32[]{:S(2)}, u32[]{:S(2)}) collective-permute-start(bf16[96,1024]{1,0:T(8,128)(2,1)} %get-tuple-element.113), channel_id=1, source_target_pairs={{0,3},{1,2},{2,1},{3,0},{4,7},{5,6},{6,5},{7,4},{8,11},{9,10},{10,... | collective-permute-start | bytes 589832 | tf_op jit(solution)/shard_map/ppermute | solution.py:334
  5.9 0.6 collective-permute-start.1
  6.6 2.1 %constant_dynamic-slice_fusion = (bf16[256,1024]{1,0:T(8,128)(2,1)}, bf16[256,1024]{1,0:T(8,128)(2,1)S(1)}) fusion(bf16[512,1024]{1,0:T(8,128)(2,1)} %param.32, s32[]{:T(128)S(6)} %select_n.200, s32[]{:T(128)S(6)} %select_n.199), kind=kLoop, calls=%fused_computation.52 | loop fusion | bytes 2097160 | tf_op jit(solution)/shard_map/dynamic_slice | solution.py:353
  8.7 3.8 %collective-permute-start.18 = (bf16[256,1024]{1,0:T(8,128)(2,1)S(1)}, bf16[256,1024]{1,0:T(8,128)(2,1)S(1)}, u32[]{:S(2)}, u32[]{:S(2)}) collective-permute-start(bf16[256,1024]{1,0:T(8,128)(2,1)S(1)} %get-tuple-element.72.refs_1_), channel_id=1, source_target_pairs={{0,4},{4,8},{8,12},{1,5},{5,9},{9,13},{2,6},{6,10},{10,14},{3,7},{... | collective-permute-start | bytes 1572872 | tf_op jit(solution)/shard_map/ppermute | solution.py:360
  12.4 1.3 collective-permute-start.19
  13.8 1.0 constant_dynamic-update-slice_fusion.3
  14.9 1.0 constant_dynamic-update-slice_fusion.2
  16.0 2.3 %constant_dynamic-update-slice_fusion.1 = bf16[1024,2048]{1,0:T(8,128)(2,1)} fusion(bf16[1024,2048]{1,0:T(8,128)(2,1)} %constant_dynamic-update-slice_fusion.2, bf16[1024,512]{1,0:T(8,128)(2,1)} %param.24), kind=kLoop, calls=%fused_computation.44 | loop fusion | bytes 2097152
  18.3 1.0 constant_dynamic-update-slice_fusion
  19.5 1.4 pad_maximum_fusion
  21.0 2.7 %collective-permute-start.3 = (bf16[96,1024]{1,0:T(8,128)(2,1)S(1)}, bf16[96,1024]{1,0:T(8,128)(2,1)S(1)}, u32[]{:S(2)}, u32[]{:S(2)}) collective-permute-start(bf16[96,1024]{1,0:T(8,128)(2,1)S(1)} %get-tuple-element.46), channel_id=1, source_target_pairs={{0,4},{4,8},{8,12},{12,0},{1,5},{5,9},{9,13},{13,1},{2,6},{6,10},{... | collective-permute-start | bytes 589832 | tf_op jit(solution)/shard_map/ppermute | solution.py:393
  23.7 3.3 %collective-permute-start.4 = (bf16[96,1024]{1,0:T(8,128)(2,1)S(1)}, bf16[96,1024]{1,0:T(8,128)(2,1)S(1)}, u32[]{:S(2)}, u32[]{:S(2)}) collective-permute-start(bf16[96,1024]{1,0:T(8,128)(2,1)S(1)} %get-tuple-element.47), channel_id=1, source_target_pairs={{0,8},{4,12},{8,0},{12,4},{1,9},{5,13},{9,1},{13,5},{2,10},{6,14},... | collective-permute-start | bytes 589832 | tf_op jit(solution)/shard_map/ppermute | solution.py:393
  26.9 0.6 collective-permute-start.5
  27.6 7.8 %collective-permute-done.3 = bf16[96,1024]{1,0:T(8,128)(2,1)S(1)} collective-permute-done((bf16[96,1024]{1,0:T(8,128)(2,1)S(1)}, bf16[96,1024]{1,0:T(8,128)(2,1)S(1)}, u32[]{:S(2)}, u32[]{:S(2)}) %collective-permute-start.3) | collective-permute-done | bytes 196640 | tf_op jit(solution)/shard_map/ppermute | solution.py:393
  35.4 7.3 %collective-permute-done.4 = bf16[96,1024]{1,0:T(8,128)(2,1)S(1)} collective-permute-done((bf16[96,1024]{1,0:T(8,128)(2,1)S(1)}, bf16[96,1024]{1,0:T(8,128)(2,1)S(1)}, u32[]{:S(2)}, u32[]{:S(2)}) %collective-permute-start.4) | collective-permute-done | bytes 196640 | tf_op jit(solution)/shard_map/ppermute | solution.py:393
  42.8 0.5 collective-permute-start.6
  43.3 0.8 collective-permute-done.7
  44.6 1.8 %fusion.17 = f32[384,2048]{1,0:T(8,128)S(1)} fusion(bf16[384,1024]{1,0:T(8,128)(2,1)S(1)} %pad_maximum_fusion.1, bf16[1024,2048]{1,0:T(8,128)(2,1)S(1)} %copy-done.11), kind=kOutput, calls=%fused_computation.79 | convolution fusion | flops 1610612736 | bytes 8126464 | tf_op jit(solution)/shard_map/dot_general | solution.py:421
  46.4 0.2 fusion.14
  46.7 5.6 %collective-permute-start.8 = (bf16[192,2048]{1,0:T(8,128)(2,1)S(1)}, bf16[192,2048]{1,0:T(8,128)(2,1)S(1)}, u32[]{:S(2)}, u32[]{:S(2)}) collective-permute-start(bf16[192,2048]{1,0:T(8,128)(2,1)S(1)} %get-tuple-element.93), channel_id=1, source_target_pairs={{0,4},{1,5},{2,6},{3,7},{16,20},{17,21},{18,22},{19,23}} | collective-permute-start | bytes 2359304 | tf_op jit(solution)/shard_map/ppermute | solution.py:444
  52.3 0.7 collective-permute-start.14
  53.0 0.7 collective-permute-start.20
  53.7 1.3 collective-permute-start.21
  55.2 1.8 %fusion.18 = f32[384,2048]{1,0:T(8,128)S(1)} fusion(bf16[384,1024]{1,0:T(8,128)(2,1)S(1)} %pad_maximum_fusion.2, bf16[1024,2048]{1,0:T(8,128)(2,1)S(1)} %copy-done.11), kind=kOutput, calls=%fused_computation.80 | convolution fusion | flops 1610612736 | bytes 8126464 | tf_op jit(solution)/shard_map/dot_general | solution.py:421
  57.1 12.7 %collective-permute-done.21.refs_6_ = bf16[256,1024]{1,0:T(8,128)(2,1)} collective-permute-done((bf16[256,1024]{1,0:T(8,128)(2,1)}, bf16[256,1024]{1,0:T(8,128)(2,1)}, u32[]{:S(2)}, u32[]{:S(2)}) %collective-permute-start.21) | collective-permute-done | bytes 524320 | tf_op jit(solution)/shard_map/ppermute | solution.py:362
  69.8 0.7 collective-permute-start.22
  70.5 1.3 collective-permute-start.23
  71.8 0.2 fusion.3
  72.0 0.2 multiply_reduce_fusion
  72.3 1.1 add_convert_fusion.3
  73.4 6.4 %collective-permute-start.13 = (bf16[192,2048]{1,0:T(8,128)(2,1)}, bf16[192,2048]{1,0:T(8,128)(2,1)}, u32[]{:S(2)}, u32[]{:S(2)}) collective-permute-start(bf16[192,2048]{1,0:T(8,128)(2,1)} %add_convert_fusion.3), channel_id=1, source_target_pairs={{0,4},{4,8},{1,5},{5,9},{2,6},{6,10},{3,7},{7,11},{16,20},{20,24},... | collective-permute-start | bytes 2359304 | tf_op jit(solution)/shard_map/ppermute | solution.py:444
  79.8 1.8 add_convert_fusion.2
  81.6 1.6 collective-permute-start.16
  83.1 1.5 collective-permute-start.10
  85.2 5.9 %take.3 = (f32[48,4,128,128]{3,2,1,0:T(8,128)}, bf16[48,4,128,128]{3,2,1,0:T(8,128)(2,1)}) custom-call(f32[48,4]{1,0:T(8,128)S(1)} %exp.16.last_ref, f32[192,128]{1,0:T(8,128)S(1)} %pad.9.aux_ref, f32[4,4,48,128]{3,2,1,0:T(8,128)S(1)} %get-tuple-element.120.key_ref, f32[4,4,48,128]{3,2,1,0:T(8,128)S(1)} %get-tuple-element.119.value_ref, ...), custom_call_target="tpu_custom_call" | custom-call | flops 67108864 | bytes 8388608 | tf_op jit(solution)/shard_map/take/pallas_call | solution.py:132
  91.1 5.8 %take.4 = (f32[48,4,128,128]{3,2,1,0:T(8,128)}, bf16[48,4,128,128]{3,2,1,0:T(8,128)(2,1)}) custom-call(f32[48,4]{1,0:T(8,128)S(1)} %exp.16.last_ref, f32[192,128]{1,0:T(8,128)S(1)} %pad.9.aux_ref, f32[4,4,48,128]{3,2,1,0:T(8,128)S(1)} %get-tuple-element.120.key_ref, ...), custom_call_target="tpu_custom_call", output_to_operand_aliasing={{0}: (5, {}), {1}: (6, {})} | custom-call | flops 67108864 | bytes 8388608 | tf_op jit(solution)/shard_map/take/pallas_call | solution.py:132
  96.9 6.0 %take.5 = (f32[48,4,128,128]{3,2,1,0:T(8,128)}, bf16[48,4,128,128]{3,2,1,0:T(8,128)(2,1)}) custom-call(f32[48,4]{1,0:T(8,128)S(1)} %exp.16.last_ref, f32[192,128]{1,0:T(8,128)S(1)} %pad.9.aux_ref, f32[4,4,48,128]{3,2,1,0:T(8,128)S(1)} %get-tuple-element.120.key_ref, ...), custom_call_target="tpu_custom_call", output_to_operand_aliasing={{0}: (5, {}), {1}: (6, {})} | custom-call | flops 67108864 | bytes 8388608 | tf_op jit(solution)/shard_map/take/pallas_call | solution.py:132
  102.9 0.7 collective-permute-start.24
  103.6 3.4 %collective-permute-start.27 = (bf16[256,1024]{1,0:T(8,128)(2,1)}, bf16[256,1024]{1,0:T(8,128)(2,1)S(1)}, u32[]{:S(2)}, u32[]{:S(2)}) collective-permute-start(bf16[256,1024]{1,0:T(8,128)(2,1)} %collective-permute-done.19.refs_5_), channel_id=1, source_target_pairs={{0,16},{4,20},{8,24},{16,0},{20,4},{24,8},{1,17},{5,21},{9,25},{17... | collective-permute-start | bytes 1572872 | tf_op jit(solution)/shard_map/ppermute | solution.py:371
  107.1 0.7 collective-permute-start.25
  107.8 2.4 %collective-permute-start.28 = (bf16[256,1024]{1,0:T(8,128)(2,1)}, bf16[256,1024]{1,0:T(8,128)(2,1)}, u32[]{:S(2)}, u32[]{:S(2)}) collective-permute-start(bf16[256,1024]{1,0:T(8,128)(2,1)} %collective-permute-done.21.refs_6_), channel_id=1, source_target_pairs={{0,16},{4,20},{16,0},{20,4},{1,17},{5,21},{17,1},{21,5},{2,18},{6,... | collective-permute-start | bytes 1572872 | tf_op jit(solution)/shard_map/ppermute | solution.py:371
  110.2 1.3 add_convert_fusion.1
  111.5 1.5 collective-permute-start.26
  113.0 1.3 add_convert_fusion
  114.3 1.0 fusion.16
  115.3 1.0 fusion.15
  116.3 3.4 %collective-permute-start.29 = (bf16[256,1024]{1,0:T(8,128)(2,1)}, bf16[256,1024]{1,0:T(8,128)(2,1)}, u32[]{:S(2)}, u32[]{:S(2)}) collective-permute-start(bf16[256,1024]{1,0:T(8,128)(2,1)} %collective-permute-done.23.refs_7_), channel_id=1, source_target_pairs={{0,16},{16,0},{1,17},{17,1},{2,18},{18,2},{3,19},{19,3}} | collective-permute-start | bytes 1572872 | tf_op jit(solution)/shard_map/ppermute | solution.py:371
  119.7 0.8 collective-permute-done.27.refs_12_
  120.5 11.0 %collective-permute-start.32 = (bf16[96,2048]{1,0:T(8,128)(2,1)}, bf16[96,2048]{1,0:T(8,128)(2,1)S(1)}, u32[]{:S(2)}, u32[]{:S(2)}) collective-permute-start(bf16[96,2048]{1,0:T(8,128)(2,1)} %get-tuple-element.99), channel_id=1, source_target_pairs={{0,4},{4,8},{8,12},{1,5},{5,9},{9,13},{2,6},{6,10},{10,14},{3,7},{... | collective-permute-start | bytes 1179656 | tf_op jit(solution)/shard_map/ppermute | solution.py:444
  131.6 1.3 collective-permute-start.33
  133.2 9.0 %collective-permute-start.15 = (bf16[96,2048]{1,0:T(8,128)(2,1)}, bf16[96,2048]{1,0:T(8,128)(2,1)S(1)}, u32[]{:S(2)}, u32[]{:S(2)}) collective-permute-start(bf16[96,2048]{1,0:T(8,128)(2,1)} %get-tuple-element.98), channel_id=1, source_target_pairs={{0,4},{4,8},{8,12},{1,5},{5,9},{9,13},{2,6},{6,10},{10,14},{3,7},{... | collective-permute-start | bytes 1179656 | tf_op jit(solution)/shard_map/ppermute | solution.py:444
  142.2 1.5 collective-permute-start.17
  143.7 6.5 %finish.3 = (bf16[96,2048]{1,0:T(8,128)(2,1)S(1)}, bf16[96,2048]{1,0:T(8,128)(2,1)S(1)}) custom-call(s32[8]{0:T(128)S(1)} %pad_add_fusion.position_ref, f32[192,128]{1,0:T(8,128)S(1)} %pad.8.aux_ref, f32[1,128]{1,0:T(1,128)S(1)} %bitcast.29, f32[192,2048]{1,0:T(8,128)} %get-tuple-element.91.own_ref, bf16[96,2048]{1,0:T(8,128)(2,1)S(1)} %collective-permute-done.32.right_ref, ...), custom_call_target="tpu_custom_call" | custom-call | flops 100663296 | bytes 3145728 | tf_op jit(solution)/shard_map/finish/pallas_call | solution.py:261
  150.3 6.5 %collective-permute-done.17.left_ref = bf16[96,2048]{1,0:T(8,128)(2,1)S(1)} collective-permute-done((bf16[96,2048]{1,0:T(8,128)(2,1)}, bf16[96,2048]{1,0:T(8,128)(2,1)S(1)}, u32[]{:S(2)}, u32[]{:S(2)}) %collective-permute-start.17) | collective-permute-done | bytes 393248 | tf_op jit(solution)/shard_map/ppermute | solution.py:444
  156.8 6.5 %finish.2 = (bf16[96,2048]{1,0:T(8,128)(2,1)S(1)}, bf16[96,2048]{1,0:T(8,128)(2,1)S(1)}) custom-call(s32[8]{0:T(128)S(1)} %pad_add_fusion.position_ref, f32[192,128]{1,0:T(8,128)S(1)} %pad.8.aux_ref, f32[1,128]{1,0:T(1,128)S(1)} %bitcast.30, f32[192,2048]{1,0:T(8,128)} %get-tuple-element.91.own_ref, bf16[96,2048]{1,0:T(8,128)(2,1)S(1)} %collective-permute-done.15.right_ref, ...), custom_call_target="tpu_custom_call" | custom-call | flops 100663296 | bytes 3145728 | tf_op jit(solution)/shard_map/finish/pallas_call | solution.py:261
  163.5 0.6 collective-permute-start.35
  164.1 0.9 collective-permute-done.30
  165.2 0.6 collective-permute-start.31
  165.8 5.5 %collective-permute-done.35 = bf16[96,1024]{1,0:T(8,128)(2,1)S(1)} collective-permute-done((bf16[96,1024]{1,0:T(8,128)(2,1)S(1)}, bf16[96,1024]{1,0:T(8,128)(2,1)S(1)}, u32[]{:S(2)}, u32[]{:S(2)}) %collective-permute-start.35) | collective-permute-done | bytes 196640 | tf_op jit(solution)/shard_map/ppermute | solution.py:334
  171.4 3.7 %collective-permute-done.31 = bf16[96,1024]{1,0:T(8,128)(2,1)S(1)} collective-permute-done((bf16[96,1024]{1,0:T(8,128)(2,1)S(1)}, bf16[96,1024]{1,0:T(8,128)(2,1)S(1)}, u32[]{:S(2)}, u32[]{:S(2)}) %collective-permute-start.31) | collective-permute-done | bytes 196640 | tf_op jit(solution)/shard_map/ppermute | solution.py:334
  175.1 0.8 pad_maximum_fusion.3
  (114 shorter events, 2.4 us)
Async XLA Ops:
  0.6 13.2 %copy-start.7 = (bf16[1024,512]{1,0:T(8,128)(2,1)S(1)}, bf16[1024,512]{1,0:T(8,128)(2,1)}, u32[]{:S(2)}) copy-start(bf16[1024,512]{1,0:T(8,128)(2,1)} %param.22) | copy-start | bytes 3145732
  2.6 12.3 %copy-start.21 = (s32[48]{0:T(128)S(1)}, s32[48]{0:T(128)}, u32[]{:S(2)}) copy-start(s32[48]{0:T(128)} %param.38) | copy-start | bytes 580
  2.6 12.3 %copy-start.8 = (bf16[1024,512]{1,0:T(8,128)(2,1)S(1)}, bf16[1024,512]{1,0:T(8,128)(2,1)}, u32[]{:S(2)}) copy-start(bf16[1024,512]{1,0:T(8,128)(2,1)} %param.23) | copy-start | bytes 3145732
  3.5 16.0 %collective-permute-start.2 = (bf16[96,1024]{1,0:T(8,128)(2,1)}, bf16[96,1024]{1,0:T(8,128)(2,1)}, u32[]{:S(2)}, u32[]{:S(2)}) collective-permute-start(bf16[96,1024]{1,0:T(8,128)(2,1)} %get-tuple-element.113), channel_id=1, source_target_pairs={{0,3},{1,2},{2,1},{3,0},{4,7},{5,6},{6,5},{7,4},{8,11},{9,10},{10,... | collective-permute-start | bytes 589832 | tf_op jit(solution)/shard_map/ppermute | solution.py:334
  5.9 13.6 %collective-permute-start.1 = (bf16[96,1024]{1,0:T(8,128)(2,1)}, bf16[96,1024]{1,0:T(8,128)(2,1)}, u32[]{:S(2)}, u32[]{:S(2)}) collective-permute-start(bf16[96,1024]{1,0:T(8,128)(2,1)} %get-tuple-element.114), channel_id=1, source_target_pairs={{0,2},{1,3},{2,0},{3,1},{4,6},{5,7},{6,4},{7,5},{8,10},{9,11},{10,... | collective-permute-start | bytes 589832 | tf_op jit(solution)/shard_map/ppermute | solution.py:334
  6.5 13.0 %collective-permute-start = (bf16[96,1024]{1,0:T(8,128)(2,1)}, bf16[96,1024]{1,0:T(8,128)(2,1)}, u32[]{:S(2)}, u32[]{:S(2)}) collective-permute-start(bf16[96,1024]{1,0:T(8,128)(2,1)} %get-tuple-element.115), channel_id=1, source_target_pairs={{0,1},{1,0},{2,3},{3,2},{4,5},{5,4},{6,7},{7,6},{8,9},{9,8},{10,11... | collective-permute-start | bytes 589832 | tf_op jit(solution)/shard_map/ppermute | solution.py:334
  8.7 43.6 %collective-permute-start.18 = (bf16[256,1024]{1,0:T(8,128)(2,1)S(1)}, bf16[256,1024]{1,0:T(8,128)(2,1)S(1)}, u32[]{:S(2)}, u32[]{:S(2)}) collective-permute-start(bf16[256,1024]{1,0:T(8,128)(2,1)S(1)} %get-tuple-element.72.refs_1_), channel_id=1, source_target_pairs={{0,4},{4,8},{8,12},{1,5},{5,9},{9,13},{2,6},{6,10},{10,14},{3,7},{... | collective-permute-start | bytes 1572872 | tf_op jit(solution)/shard_map/ppermute | solution.py:360
  12.4 40.6 %collective-permute-start.19 = (bf16[256,1024]{1,0:T(8,128)(2,1)S(1)}, bf16[256,1024]{1,0:T(8,128)(2,1)}, u32[]{:S(2)}, u32[]{:S(2)}) collective-permute-start(bf16[256,1024]{1,0:T(8,128)(2,1)S(1)} %get-tuple-element.72.refs_1_), channel_id=1, source_target_pairs={{4,0},{8,4},{12,8},{5,1},{9,5},{13,9},{6,2},{10,6},{14,10},{7,3},{... | collective-permute-start | bytes 1572872 | tf_op jit(solution)/shard_map/ppermute | solution.py:362
  14.8 3.4 %copy-start.9 = (bf16[1024,512]{1,0:T(8,128)(2,1)S(1)}, bf16[1024,512]{1,0:T(8,128)(2,1)}, u32[]{:S(2)}) copy-start(bf16[1024,512]{1,0:T(8,128)(2,1)} %param.25) | copy-start | bytes 3145732
  14.9 4.4 %copy-start.16 = (f32[48,4,4]{0,2,1:T(4,128)S(1)}, f32[48,4,4]{0,2,1:T(4,128)}, u32[]{:S(2)}) copy-start(f32[48,4,4]{0,2,1:T(4,128)} %param.37) | copy-start | bytes 9220
  14.9 4.4 %copy-start.17 = (f32[48,4,4]{0,2,1:T(4,128)S(1)}, f32[48,4,4]{0,2,1:T(4,128)}, u32[]{:S(2)}) copy-start(f32[48,4,4]{0,2,1:T(4,128)} %param.36) | copy-start | bytes 9220
  14.9 4.5 %copy-start.12 = (bf16[48,4,4,128]{3,2,1,0:T(4,128)(2,1)S(1)}, bf16[48,4,4,128]{3,2,1,0:T(4,128)(2,1)}, u32[]{:S(2)}) copy-start(bf16[48,4,4,128]{3,2,1,0:T(4,128)(2,1)} %param.35) | copy-start | bytes 589828
  14.9 4.5 %copy-start.13 = (bf16[48,4,4,128]{3,2,1,0:T(4,128)(2,1)S(1)}, bf16[48,4,4,128]{3,2,1,0:T(4,128)(2,1)}, u32[]{:S(2)}) copy-start(bf16[48,4,4,128]{3,2,1,0:T(4,128)(2,1)} %param.34) | copy-start | bytes 589828
  16.0 3.5 %copy-start.10 = (bf16[1,96,1024]{2,1,0:T(8,128)(2,1)S(1)}, bf16[1,96,1024]{2,1,0:T(8,128)(2,1)}, u32[]{:S(2)}) copy-start(bf16[1,96,1024]{2,1,0:T(8,128)(2,1)} %get-tuple-element.112) | copy-start | bytes 589828
  18.3 9.3 %copy-start.20 = (s32[7]{0:T(128)S(1)}, s32[7]{0:T(128)}, u32[]{:S(2)}) copy-start(s32[7]{0:T(128)} %constant.185.clone) | copy-start | bytes 88
  18.3 24.5 %copy-start.22 = (f32[4]{0:T(128)S(1)}, f32[4]{0:T(128)}, u32[]{:S(2)}) copy-start(f32[4]{0:T(128)} %param.28) | copy-start | bytes 52
  19.5 25.1 %copy-start.11 = (bf16[1024,2048]{1,0:T(8,128)(2,1)S(1)}, bf16[1024,2048]{1,0:T(8,128)(2,1)}, u32[]{:S(2)}) copy-start(bf16[1024,2048]{1,0:T(8,128)(2,1)} %constant_dynamic-update-slice_fusion) | copy-start | bytes 12582916
  21.0 14.5 %collective-permute-start.3 = (bf16[96,1024]{1,0:T(8,128)(2,1)S(1)}, bf16[96,1024]{1,0:T(8,128)(2,1)S(1)}, u32[]{:S(2)}, u32[]{:S(2)}) collective-permute-start(bf16[96,1024]{1,0:T(8,128)(2,1)S(1)} %get-tuple-element.46), channel_id=1, source_target_pairs={{0,4},{4,8},{8,12},{12,0},{1,5},{5,9},{9,13},{13,1},{2,6},{6,10},{... | collective-permute-start | bytes 589832 | tf_op jit(solution)/shard_map/ppermute | solution.py:393
  23.7 19.1 %collective-permute-start.4 = (bf16[96,1024]{1,0:T(8,128)(2,1)S(1)}, bf16[96,1024]{1,0:T(8,128)(2,1)S(1)}, u32[]{:S(2)}, u32[]{:S(2)}) collective-permute-start(bf16[96,1024]{1,0:T(8,128)(2,1)S(1)} %get-tuple-element.47), channel_id=1, source_target_pairs={{0,8},{4,12},{8,0},{12,4},{1,9},{5,13},{9,1},{13,5},{2,10},{6,14},... | collective-permute-start | bytes 589832 | tf_op jit(solution)/shard_map/ppermute | solution.py:393
  26.9 15.8 %collective-permute-start.5 = (bf16[96,1024]{1,0:T(8,128)(2,1)S(1)}, bf16[96,1024]{1,0:T(8,128)(2,1)S(1)}, u32[]{:S(2)}, u32[]{:S(2)}) collective-permute-start(bf16[96,1024]{1,0:T(8,128)(2,1)S(1)} %get-tuple-element.48), channel_id=1, source_target_pairs={{0,12},{4,0},{8,4},{12,8},{1,13},{5,1},{9,5},{13,9},{2,14},{6,2},{... | collective-permute-start | bytes 589832 | tf_op jit(solution)/shard_map/ppermute | solution.py:393
  42.7 1.4 collective-permute-start.7
  42.8 1.7 collective-permute-start.6
  43.3 10.5 %collective-permute-start.12 = (bf16[96,1024]{1,0:T(8,128)(2,1)S(1)}, bf16[96,1024]{1,0:T(8,128)(2,1)S(1)}, u32[]{:S(2)}, u32[]{:S(2)}) collective-permute-start(bf16[96,1024]{1,0:T(8,128)(2,1)S(1)} %collective-permute-done.4), channel_id=1, source_target_pairs={{0,1},{1,0},{2,3},{3,2},{4,5},{5,4},{6,7},{7,6},{8,9},{9,8},{10,11... | collective-permute-start | bytes 589832 | tf_op jit(solution)/shard_map/ppermute | solution.py:334
  44.2 10.9 %collective-permute-start.11 = (bf16[96,1024]{1,0:T(8,128)(2,1)S(1)}, bf16[96,1024]{1,0:T(8,128)(2,1)S(1)}, u32[]{:S(2)}, u32[]{:S(2)}) collective-permute-start(bf16[96,1024]{1,0:T(8,128)(2,1)S(1)} %get-tuple-element.54), channel_id=1, source_target_pairs={{0,1},{1,0},{2,3},{3,2},{4,5},{5,4},{6,7},{7,6},{8,9},{9,8},{10,11... | collective-permute-start | bytes 589832 | tf_op jit(solution)/shard_map/ppermute | solution.py:334
  46.4 8.8 %copy-start.1 = (f32[384,2048]{1,0:T(8,128)}, f32[384,2048]{1,0:T(8,128)S(1)}, u32[]{:S(2)}) copy-start(f32[384,2048]{1,0:T(8,128)S(1)} %fusion.17) | copy-start | bytes 9437188
  46.7 25.1 %collective-permute-start.8 = (bf16[192,2048]{1,0:T(8,128)(2,1)S(1)}, bf16[192,2048]{1,0:T(8,128)(2,1)S(1)}, u32[]{:S(2)}, u32[]{:S(2)}) collective-permute-start(bf16[192,2048]{1,0:T(8,128)(2,1)S(1)} %get-tuple-element.93), channel_id=1, source_target_pairs={{0,4},{1,5},{2,6},{3,7},{16,20},{17,21},{18,22},{19,23}} | collective-permute-start | bytes 2359304 | tf_op jit(solution)/shard_map/ppermute | solution.py:444
  52.3 27.5 %collective-permute-start.14 = (bf16[192,2048]{1,0:T(8,128)(2,1)S(1)}, bf16[192,2048]{1,0:T(8,128)(2,1)S(1)}, u32[]{:S(2)}, u32[]{:S(2)}) collective-permute-start(bf16[192,2048]{1,0:T(8,128)(2,1)S(1)} %get-tuple-element.92), channel_id=1, source_target_pairs={{12,8},{13,9},{14,10},{15,11},{28,24},{29,25},{30,26},{31,27}} | collective-permute-start | bytes 2359304 | tf_op jit(solution)/shard_map/ppermute | solution.py:444
  53.0 4.1 %collective-permute-start.20 = (bf16[256,1024]{1,0:T(8,128)(2,1)S(1)}, bf16[256,1024]{1,0:T(8,128)(2,1)S(1)}, u32[]{:S(2)}, u32[]{:S(2)}) collective-permute-start(bf16[256,1024]{1,0:T(8,128)(2,1)S(1)} %collective-permute-done.18.refs_2_), channel_id=1, source_target_pairs={{4,8},{8,12},{5,9},{9,13},{6,10},{10,14},{7,11},{11,15},{20,24},{2... | collective-permute-start | bytes 1572872 | tf_op jit(solution)/shard_map/ppermute | solution.py:360
  53.7 16.0 %collective-permute-start.21 = (bf16[256,1024]{1,0:T(8,128)(2,1)}, bf16[256,1024]{1,0:T(8,128)(2,1)}, u32[]{:S(2)}, u32[]{:S(2)}) collective-permute-start(bf16[256,1024]{1,0:T(8,128)(2,1)} %collective-permute-done.19.refs_5_), channel_id=1, source_target_pairs={{4,0},{8,4},{5,1},{9,5},{6,2},{10,6},{7,3},{11,7},{20,16},{24,20},... | collective-permute-start | bytes 1572872 | tf_op jit(solution)/shard_map/ppermute | solution.py:362
  55.2 16.6 %copy-start.14 = (bf16[4096,16]{0,1:T(8,128)(2,1)S(1)}, bf16[4096,16]{0,1:T(8,128)(2,1)}, u32[]{:S(2)}) copy-start(bf16[4096,16]{0,1:T(8,128)(2,1)} %param.26) | copy-start | bytes 393220
  55.2 16.6 %copy-start.15 = (bf16[4096,16]{0,1:T(8,128)(2,1)S(1)}, bf16[4096,16]{0,1:T(8,128)(2,1)}, u32[]{:S(2)}) copy-start(bf16[4096,16]{0,1:T(8,128)(2,1)} %param.27) | copy-start | bytes 393220
  55.2 16.8 %copy-start.6 = (bf16[192,1024]{1,0:T(8,128)(2,1)S(1)}, bf16[192,1024]{1,0:T(8,128)(2,1)}, u32[]{:S(2)}) copy-start(bf16[192,1024]{1,0:T(8,128)(2,1)} %param.20) | copy-start | bytes 1179652
  69.8 33.8 %collective-permute-start.22 = (bf16[256,1024]{1,0:T(8,128)(2,1)S(1)}, bf16[256,1024]{1,0:T(8,128)(2,1)S(1)}, u32[]{:S(2)}, u32[]{:S(2)}) collective-permute-start(bf16[256,1024]{1,0:T(8,128)(2,1)S(1)} %collective-permute-done.20.refs_3_), channel_id=1, source_target_pairs={{8,12},{9,13},{10,14},{11,15},{24,28},{25,29},{26,30},{27,31}} | collective-permute-start | bytes 1572872 | tf_op jit(solution)/shard_map/ppermute | solution.py:360
  70.5 36.6 %collective-permute-start.23 = (bf16[256,1024]{1,0:T(8,128)(2,1)}, bf16[256,1024]{1,0:T(8,128)(2,1)}, u32[]{:S(2)}, u32[]{:S(2)}) collective-permute-start(bf16[256,1024]{1,0:T(8,128)(2,1)} %collective-permute-done.21.refs_6_), channel_id=1, source_target_pairs={{4,0},{5,1},{6,2},{7,3},{20,16},{21,17},{22,18},{23,19}} | collective-permute-start | bytes 1572872 | tf_op jit(solution)/shard_map/ppermute | solution.py:362
  72.2 10.9 %collective-permute-start.9 = (f32[192,33]{0,1:T(8,128)S(1)}, f32[192,33]{0,1:T(8,128)S(1)}, u32[]{:S(2)}, u32[]{:S(2)}) collective-permute-start(f32[192,33]{0,1:T(8,128)S(1)} %pad_maximum_fusion.4), channel_id=1, source_target_pairs={{0,1},{1,0},{2,3},{3,2},{4,5},{5,4},{6,7},{7,6},{8,9},{9,8},{10,11... | collective-permute-start | bytes 76040 | tf_op jit(solution)/shard_map/ppermute | solution.py:491
  73.4 11.3 %copy-start.18 = (f32[48,4,4]{0,2,1:T(4,128)S(1)}, f32[48,4,4]{0,2,1:T(4,128)}, u32[]{:S(2)}) copy-start(f32[48,4,4]{0,2,1:T(4,128)} %param.30) | copy-start | bytes 9220
  73.4 34.3 %collective-permute-start.13 = (bf16[192,2048]{1,0:T(8,128)(2,1)}, bf16[192,2048]{1,0:T(8,128)(2,1)}, u32[]{:S(2)}, u32[]{:S(2)}) collective-permute-start(bf16[192,2048]{1,0:T(8,128)(2,1)} %add_convert_fusion.3), channel_id=1, source_target_pairs={{0,4},{4,8},{1,5},{5,9},{2,6},{6,10},{3,7},{7,11},{16,20},{20,24},... | collective-permute-start | bytes 2359304 | tf_op jit(solution)/shard_map/ppermute | solution.py:444
  81.6 30.0 %collective-permute-start.16 = (bf16[192,2048]{1,0:T(8,128)(2,1)}, bf16[192,2048]{1,0:T(8,128)(2,1)}, u32[]{:S(2)}, u32[]{:S(2)}) collective-permute-start(bf16[192,2048]{1,0:T(8,128)(2,1)} %get-tuple-element.90), channel_id=1, source_target_pairs={{8,4},{12,8},{9,5},{13,9},{10,6},{14,10},{11,7},{15,11},{24,20},{2... | collective-permute-start | bytes 2359304 | tf_op jit(solution)/shard_map/ppermute | solution.py:444
  83.1 19.8 %collective-permute-start.10 = (f32[192,33]{0,1:T(8,128)S(1)}, f32[192,33]{0,1:T(8,128)S(1)}, u32[]{:S(2)}, u32[]{:S(2)}) collective-permute-start(f32[192,33]{0,1:T(8,128)S(1)} %fusion.12), channel_id=1, source_target_pairs={{0,2},{1,3},{2,0},{3,1},{4,6},{5,7},{6,4},{7,5},{8,10},{9,11},{10,... | collective-permute-start | bytes 76040 | tf_op jit(solution)/shard_map/ppermute | solution.py:491
  96.9 13.3 %copy-start.2 = (f32[384,2048]{1,0:T(8,128)S(1)}, f32[384,2048]{1,0:T(8,128)}, u32[]{:S(2)}) copy-start(f32[384,2048]{1,0:T(8,128)} %copy-done.1) | copy-start | bytes 9437188
  102.9 13.4 %collective-permute-start.24 = (bf16[256,1024]{1,0:T(8,128)(2,1)S(1)}, bf16[256,1024]{1,0:T(8,128)(2,1)S(1)}, u32[]{:S(2)}, u32[]{:S(2)}) collective-permute-start(bf16[256,1024]{1,0:T(8,128)(2,1)S(1)} %collective-permute-done.18.refs_2_), channel_id=1, source_target_pairs={{4,20},{8,24},{12,28},{20,4},{24,8},{28,12},{5,21},{9,25},{13,29},... | collective-permute-start | bytes 1572872 | tf_op jit(solution)/shard_map/ppermute | solution.py:370
  103.6 16.9 %collective-permute-start.27 = (bf16[256,1024]{1,0:T(8,128)(2,1)}, bf16[256,1024]{1,0:T(8,128)(2,1)S(1)}, u32[]{:S(2)}, u32[]{:S(2)}) collective-permute-start(bf16[256,1024]{1,0:T(8,128)(2,1)} %collective-permute-done.19.refs_5_), channel_id=1, source_target_pairs={{0,16},{4,20},{8,24},{16,0},{20,4},{24,8},{1,17},{5,21},{9,25},{17... | collective-permute-start | bytes 1572872 | tf_op jit(solution)/shard_map/ppermute | solution.py:371
  107.1 24.5 %collective-permute-start.25 = (bf16[256,1024]{1,0:T(8,128)(2,1)S(1)}, bf16[256,1024]{1,0:T(8,128)(2,1)S(1)}, u32[]{:S(2)}, u32[]{:S(2)}) collective-permute-start(bf16[256,1024]{1,0:T(8,128)(2,1)S(1)} %collective-permute-done.20.refs_3_), channel_id=1, source_target_pairs={{8,24},{12,28},{24,8},{28,12},{9,25},{13,29},{25,9},{29,13},{10,26... | collective-permute-start | bytes 1572872 | tf_op jit(solution)/shard_map/ppermute | solution.py:370
  107.8 25.4 %collective-permute-start.28 = (bf16[256,1024]{1,0:T(8,128)(2,1)}, bf16[256,1024]{1,0:T(8,128)(2,1)}, u32[]{:S(2)}, u32[]{:S(2)}) collective-permute-start(bf16[256,1024]{1,0:T(8,128)(2,1)} %collective-permute-done.21.refs_6_), channel_id=1, source_target_pairs={{0,16},{4,20},{16,0},{20,4},{1,17},{5,21},{17,1},{21,5},{2,18},{6,... | collective-permute-start | bytes 1572872 | tf_op jit(solution)/shard_map/ppermute | solution.py:371
  111.5 21.4 %copy-start.19 = (f32[4]{0:T(128)S(1)}, f32[4]{0:T(128)}, u32[]{:S(2)}) copy-start(f32[4]{0:T(128)} %param.29) | copy-start | bytes 52
  111.5 32.2 %copy-start = (f32[128]{0:T(128)S(1)}, f32[128]{0:T(128)}, u32[]{:S(2)}) copy-start(f32[128]{0:T(128)} %param.31) | copy-start | bytes 1540
  111.5 30.6 %collective-permute-start.26 = (bf16[256,1024]{1,0:T(8,128)(2,1)S(1)}, bf16[256,1024]{1,0:T(8,128)(2,1)}, u32[]{:S(2)}, u32[]{:S(2)}) collective-permute-start(bf16[256,1024]{1,0:T(8,128)(2,1)S(1)} %collective-permute-done.22.refs_4_), channel_id=1, source_target_pairs={{12,28},{28,12},{13,29},{29,13},{14,30},{30,14},{15,31},{31,15}} | collective-permute-start | bytes 1572872 | tf_op jit(solution)/shard_map/ppermute | solution.py:370
  116.3 15.3 %copy-start.3 = (bf16[256,1024]{1,0:T(8,128)(2,1)}, bf16[256,1024]{1,0:T(8,128)(2,1)S(1)}, u32[]{:S(2)}) copy-start(bf16[256,1024]{1,0:T(8,128)(2,1)S(1)} %collective-permute-done.24.refs_9_) | copy-start | bytes 1572868
  116.3 27.3 %collective-permute-start.29 = (bf16[256,1024]{1,0:T(8,128)(2,1)}, bf16[256,1024]{1,0:T(8,128)(2,1)}, u32[]{:S(2)}, u32[]{:S(2)}) collective-permute-start(bf16[256,1024]{1,0:T(8,128)(2,1)} %collective-permute-done.23.refs_7_), channel_id=1, source_target_pairs={{0,16},{16,0},{1,17},{17,1},{2,18},{18,2},{3,19},{19,3}} | collective-permute-start | bytes 1572872 | tf_op jit(solution)/shard_map/ppermute | solution.py:371
  120.5 12.4 %copy-start.4 = (bf16[256,1024]{1,0:T(8,128)(2,1)}, bf16[256,1024]{1,0:T(8,128)(2,1)S(1)}, u32[]{:S(2)}) copy-start(bf16[256,1024]{1,0:T(8,128)(2,1)S(1)} %collective-permute-done.27.refs_12_) | copy-start | bytes 1572868
  120.5 23.1 %collective-permute-start.32 = (bf16[96,2048]{1,0:T(8,128)(2,1)}, bf16[96,2048]{1,0:T(8,128)(2,1)S(1)}, u32[]{:S(2)}, u32[]{:S(2)}) collective-permute-start(bf16[96,2048]{1,0:T(8,128)(2,1)} %get-tuple-element.99), channel_id=1, source_target_pairs={{0,4},{4,8},{8,12},{1,5},{5,9},{9,13},{2,6},{6,10},{10,14},{3,7},{... | collective-permute-start | bytes 1179656 | tf_op jit(solution)/shard_map/ppermute | solution.py:444
  131.6 1.3 copy-start.5
  131.6 12.1 %collective-permute-start.33 = (bf16[96,2048]{1,0:T(8,128)(2,1)}, bf16[96,2048]{1,0:T(8,128)(2,1)S(1)}, u32[]{:S(2)}, u32[]{:S(2)}) collective-permute-start(bf16[96,2048]{1,0:T(8,128)(2,1)} %get-tuple-element.97), channel_id=1, source_target_pairs={{4,0},{8,4},{12,8},{5,1},{9,5},{13,9},{6,2},{10,6},{14,10},{7,3},{... | collective-permute-start | bytes 1179656 | tf_op jit(solution)/shard_map/ppermute | solution.py:444
  133.2 17.1 %collective-permute-start.15 = (bf16[96,2048]{1,0:T(8,128)(2,1)}, bf16[96,2048]{1,0:T(8,128)(2,1)S(1)}, u32[]{:S(2)}, u32[]{:S(2)}) collective-permute-start(bf16[96,2048]{1,0:T(8,128)(2,1)} %get-tuple-element.98), channel_id=1, source_target_pairs={{0,4},{4,8},{8,12},{1,5},{5,9},{9,13},{2,6},{6,10},{10,14},{3,7},{... | collective-permute-start | bytes 1179656 | tf_op jit(solution)/shard_map/ppermute | solution.py:444
  142.2 14.7 %collective-permute-start.17 = (bf16[96,2048]{1,0:T(8,128)(2,1)}, bf16[96,2048]{1,0:T(8,128)(2,1)S(1)}, u32[]{:S(2)}, u32[]{:S(2)}) collective-permute-start(bf16[96,2048]{1,0:T(8,128)(2,1)} %get-tuple-element.96), channel_id=1, source_target_pairs={{4,0},{8,4},{12,8},{5,1},{9,5},{13,9},{6,2},{10,6},{14,10},{7,3},{... | collective-permute-start | bytes 1179656 | tf_op jit(solution)/shard_map/ppermute | solution.py:444
  150.2 13.2 %collective-permute-start.34 = (bf16[96,2048]{1,0:T(8,128)(2,1)S(1)}, bf16[96,2048]{1,0:T(8,128)(2,1)S(1)}, u32[]{:S(2)}, u32[]{:S(2)}) collective-permute-start(bf16[96,2048]{1,0:T(8,128)(2,1)S(1)} %get-tuple-element.86), channel_id=1, source_target_pairs={{0,1},{1,0},{2,3},{3,2},{4,5},{5,4},{6,7},{7,6},{8,9},{9,8},{10,11... | collective-permute-start | bytes 1179656 | tf_op jit(solution)/shard_map/ppermute | solution.py:334
  163.3 1.8 %collective-permute-start.30 = (bf16[96,2048]{1,0:T(8,128)(2,1)S(1)}, bf16[96,2048]{1,0:T(8,128)(2,1)S(1)}, u32[]{:S(2)}, u32[]{:S(2)}) collective-permute-start(bf16[96,2048]{1,0:T(8,128)(2,1)S(1)} %get-tuple-element.84), channel_id=1, source_target_pairs={{0,1},{1,0},{2,3},{3,2},{4,5},{5,4},{6,7},{7,6},{8,9},{9,8},{10,11... | collective-permute-start | bytes 1179656 | tf_op jit(solution)/shard_map/ppermute | solution.py:334
  163.5 7.8 %collective-permute-start.35 = (bf16[96,1024]{1,0:T(8,128)(2,1)S(1)}, bf16[96,1024]{1,0:T(8,128)(2,1)S(1)}, u32[]{:S(2)}, u32[]{:S(2)}) collective-permute-start(bf16[96,1024]{1,0:T(8,128)(2,1)S(1)} %slice.88), channel_id=1, source_target_pairs={{0,2},{1,3},{2,0},{3,1},{4,6},{5,7},{6,4},{7,5},{8,10},{9,11},{10,... | collective-permute-start | bytes 589832 | tf_op jit(solution)/shard_map/ppermute | solution.py:334
  165.2 9.9 %collective-permute-start.31 = (bf16[96,1024]{1,0:T(8,128)(2,1)S(1)}, bf16[96,1024]{1,0:T(8,128)(2,1)S(1)}, u32[]{:S(2)}, u32[]{:S(2)}) collective-permute-start(bf16[96,1024]{1,0:T(8,128)(2,1)S(1)} %slice.89), channel_id=1, source_target_pairs={{0,2},{1,3},{2,0},{3,1},{4,6},{5,7},{6,4},{7,5},{8,10},{9,11},{10,... | collective-permute-start | bytes 589832 | tf_op jit(solution)/shard_map/ppermute | solution.py:334
where the time goes:
time: 178 us; the launch traced here: 176 us
  starting transfers between devices  71.6 us (40%)
  waiting for transfers between devices  46.3 us (26%)
  Pallas kernels  30.7 us (17%)
  local copies, waits for them, and re-layouts  12.2 us (7%)
  other arithmetic  9.68 us (5%)
  matrix products  3.88 us (2%)
    ppermute x8, starting transfers between devices, on_device(): both.append(lax.ppermute(send, 'kv', places[side]))  37 us
    pallas_call x3, Pallas kernels, take(): pl.pallas_call(functools.partial(take_kernel, start), grid=(steps,), in_s...  17.7 us
    ppermute x3, waiting for transfers between devices, on_device(): lax.ppermute(sends[k], 'kv', [(i, (i + k) % n_kv) for i in range(n_kv)])  15.2 us
    pallas_call x2, Pallas kernels, finish(): pl.pallas_call(functools.partial(finish_kernel, n_refs), grid=(steps,), i...  13 us
    ppermute x3, waiting for transfers between devices, weight_round(): lefts.append(lax.ppermute(left, 'kv', pairs))  12.7 us
    ppermute x11, waiting for transfers between devices, swap(): return lax.ppermute(value, 'tp', [(i, i ^ mask) for i in range(n_tp)])  11.1 us
    ppermute x3, starting transfers between devices, weight_cross(): far_lefts.append(lax.ppermute(left, both, pairs(range(n_kv - i))))  9.26 us
    ppermute x3, starting transfers between devices, on_device(): lax.ppermute(sends[k], 'kv', [(i, (i + k) % n_kv) for i in range(n_kv)])  6.6 us
  transfers between devices with their start and end apart: 36, of which 11 were waited for; matrix products, arithmetic and copies ran while one was open for 13% of the time, Pallas kernels for 17%

commit v1 on v0

--- a/solution.py
+++ b/solution.py
@@ -386,7 +386,8 @@
                 (1, part_rows, kv_cols),
             )[0]
 
-        sends = lax.optimization_barrier(tuple(block_for((z + k) % n_kv) for k in range(n_kv)))
+        sends = [block_for((z + k) % n_kv) for k in range(n_kv)]
+        *sends, joined = lax.optimization_barrier((*sends, joined))
         received.append(
             [sends[0]]
             + [
@@ -445,14 +446,9 @@
                 got.append(tuple(both))
             arrived[chunk] = got
             if chunk == 0:
-                if 2 * i < n_kv:
-                    weight_round(2 * i, token)
-                for q in range(max(2 * i - 2, 1), min(2 * i, n_kv)):
-                    weight_cross(q)
-                if 2 * i + 1 < n_kv:
-                    weight_round(2 * i + 1, token)
-        if i == 1:
-            first_arrived = arrived[0][0][0]
+                if i + 1 < n_kv:
+                    weight_round(i + 1, token)
+                weight_cross(i)
 
     early = lax.optimization_barrier(
         (
@@ -477,18 +473,17 @@
 
     small = jnp.concatenate([forgetting_projector, strength_projector_matrix], axis=1)
     small = lax.dynamic_slice_in_dim(small, tp * local_cols, local_cols)
-    tied, raw = lax.optimization_barrier((gained, candidate_embeddings, first_arrived))[:2]
-    raw = raw.astype(f32)
+    raw = candidate_embeddings.astype(f32)
     sums = jnp.concatenate(
         [
-            jnp.dot(tied, small, preferred_element_type=f32),
+            jnp.dot(gained, small, preferred_element_type=f32),
             jnp.sum(raw * raw, axis=1, keepdims=True),
         ],
         axis=1,
     )
     mask = 1
     while mask < n_tp:
-        sums = sums + lax.ppermute(sums, "tp", [(i, i ^ mask) for i in range(n_tp)])
+        sums = sums + swap(sums, mask)
         mask *= 2
     scale = lax.rsqrt(sums[:, 2 * all_heads :] / model + epsilon)
     own = lambda at: lax.dynamic_slice_in_dim(sums, at + tp * heads, heads, 1) * scale

time: 178 us -> 176 us (0.989)
  local copies, waits for them, and re-layouts: 12.2 us -> 5.44 us
  starting transfers between devices: 71.6 us -> 75.5 us
  waiting for transfers between devices: 46.3 us -> 42.5 us
  other arithmetic: 9.68 us -> 12.7 us
    ppermute x3, waiting for transfers between devices: 12.7 us -> 0.01 us  [weight_round(): lefts.append(lax.ppermute(left, 'kv', pairs))]
    ppermute x8, waiting for transfers between devices: 6.57 us -> 18.1 us  [on_device(): both.append(lax.ppermute(send, 'kv', places[side]))]
    unnamed x50 -> x35, local copies, waits for them, and re-layouts: 4.63 us -> 0.19 us
    ppermute x3, waiting for transfers between devices: 15.2 us -> 11 us  [on_device(): lax.ppermute(sends[k], 'kv', [(i, (i + k) % n_kv) for i in range(n_kv)])]
    ppermute x8, starting transfers between devices: 37 us -> 41.1 us  [on_device(): both.append(lax.ppermute(send, 'kv', places[side]))]
    concatenate x1 -> x2, other arithmetic: 0.01 us -> 2.14 us  [the longest x1 2.13 us: on_device(): jnp.concatenate([probe_projector, address_projector, content_projector, s...]
    ppermute x11 -> x13, starting transfers between devices: 5.2 us -> 7.24 us  [swap(): return lax.ppermute(value, 'tp', [(i, i ^ mask) for i in range(n_tp)])]
    ppermute x11 -> x13, waiting for transfers between devices: 11.1 us -> 12.8 us  [swap(): return lax.ppermute(value, 'tp', [(i, i ^ mask) for i in range(n_tp)])]
  transfers between devices with their start and end apart: 36 -> 36, of which waited for: 11 -> 13; matrix products, arithmetic and copies ran while one was open for 13% -> 11% of each run, Pallas kernels for 17% -> 18%
where the time goes in v1:
time: 176 us; the launch traced here: 173 us
  starting transfers between devices  75.5 us (43%)
  waiting for transfers between devices  42.5 us (24%)
  Pallas kernels  30.7 us (17%)
  other arithmetic  12.7 us (7%)
  local copies, waits for them, and re-layouts  5.44 us (3%)
  matrix products  4.68 us (3%)
    ppermute x8, starting transfers between devices, on_device(): both.append(lax.ppermute(send, 'kv', places[side]))  41.1 us
    ppermute x8, waiting for transfers between devices, on_device(): both.append(lax.ppermute(send, 'kv', places[side]))  18.1 us
    pallas_call x3, Pallas kernels, take(): pl.pallas_call(functools.partial(take_kernel, start), grid=(steps,), in_s...  17.8 us
    pallas_call x2, Pallas kernels, finish(): pl.pallas_call(functools.partial(finish_kernel, n_refs), grid=(steps,), i...  12.9 us
    ppermute x13, waiting for transfers between devices, swap(): return lax.ppermute(value, 'tp', [(i, i ^ mask) for i in range(n_tp)])  12.8 us
    ppermute x3, waiting for transfers between devices, on_device(): lax.ppermute(sends[k], 'kv', [(i, (i + k) % n_kv) for i in range(n_kv)])  11 us
    ppermute x3, starting transfers between devices, weight_cross(): far_lefts.append(lax.ppermute(left, both, pairs(range(n_kv - i))))  9.26 us
    ppermute x13, starting transfers between devices, swap(): return lax.ppermute(value, 'tp', [(i, i ^ mask) for i in range(n_tp)])  7.24 us
  transfers between devices with their start and end apart: 36, of which 13 were waited for; matrix products, arithmetic and copies ran while one was open for 11% of the time, Pallas kernels for 18%

profile of v1, /device:TPU:0, one launch (start us, length us, event | category | flops | bytes accessed | tf_op | source)
XLA Modules:
  0.0 172.9 jit_solution(15163299362896496273)
XLA Ops:
  0.6 0.8 dynamic_slice.46
  1.4 1.2 fusion
  2.6 1.1 fusion.5
  3.7 0.6 collective-permute-start
  4.3 0.8 dynamic-slice_bitcast_fusion.4
  5.1 2.6 %collective-permute-start.4 = (bf16[96,1024]{1,0:T(8,128)(2,1)}, bf16[96,1024]{1,0:T(8,128)(2,1)}, u32[]{:S(2)}, u32[]{:S(2)}) collective-permute-start(bf16[96,1024]{1,0:T(8,128)(2,1)} %get-tuple-element.111), channel_id=1, source_target_pairs={{0,3},{1,2},{2,1},{3,0},{4,7},{5,6},{6,5},{7,4},{8,11},{9,10},{10,... | collective-permute-start | bytes 589832 | tf_op jit(solution)/shard_map/ppermute | solution.py:334
  7.8 0.9 constant_dynamic-slice_fusion
  8.7 3.9 %collective-permute-start.18 = (bf16[256,1024]{1,0:T(8,128)(2,1)S(1)}, bf16[256,1024]{1,0:T(8,128)(2,1)S(1)}, u32[]{:S(2)}, u32[]{:S(2)}) collective-permute-start(bf16[256,1024]{1,0:T(8,128)(2,1)S(1)} %get-tuple-element.70.refs_1_), channel_id=1, source_target_pairs={{0,4},{4,8},{8,12},{1,5},{5,9},{9,13},{2,6},{6,10},{10,14},{3,7},{... | collective-permute-start | bytes 1572872 | tf_op jit(solution)/shard_map/ppermute | solution.py:360
  12.7 1.1 convert_bitcast_fusion
  13.8 2.1 %pad_maximum_fusion = bf16[1024,2048]{1,0:T(8,128)(2,1)S(1)} fusion(bf16[1024,512]{1,0:T(8,128)(2,1)S(1)} %copy-done.9, bf16[1024,512]{1,0:T(8,128)(2,1)} %param.24, bf16[1024,512]{1,0:T(8,128)(2,1)} %param.23, bf16[1024,512]{1,0:T(8,128)(2,1)} %param.22), kind=kLoop, calls=%fused_computation | loop fusion | flops 16777216 | bytes 8388608 | tf_op jit(solution)/shard_map/concatenate | solution.py:375
  16.0 1.6 collective-permute-done.3
  17.7 1.2 pad_maximum_fusion.1
  19.0 1.9 %collective-permute-start.5 = (bf16[96,1024]{1,0:T(8,128)(2,1)S(1)}, bf16[96,1024]{1,0:T(8,128)(2,1)S(1)}, u32[]{:S(2)}, u32[]{:S(2)}) collective-permute-start(bf16[96,1024]{1,0:T(8,128)(2,1)S(1)} %get-tuple-element.45), channel_id=1, source_target_pairs={{0,4},{4,8},{8,12},{12,0},{1,5},{5,9},{9,13},{13,1},{2,6},{6,10},{... | collective-permute-start | bytes 589832 | tf_op jit(solution)/shard_map/ppermute | solution.py:394
  20.9 2.6 %collective-permute-start.6 = (bf16[96,1024]{1,0:T(8,128)(2,1)S(1)}, bf16[96,1024]{1,0:T(8,128)(2,1)S(1)}, u32[]{:S(2)}, u32[]{:S(2)}) collective-permute-start(bf16[96,1024]{1,0:T(8,128)(2,1)S(1)} %get-tuple-element.46), channel_id=1, source_target_pairs={{0,8},{4,12},{8,0},{12,4},{1,9},{5,13},{9,1},{13,5},{2,10},{6,14},... | collective-permute-start | bytes 589832 | tf_op jit(solution)/shard_map/ppermute | solution.py:394
  23.4 1.3 collective-permute-start.7
  24.8 4.3 %collective-permute-done.5 = bf16[96,1024]{1,0:T(8,128)(2,1)S(1)} collective-permute-done((bf16[96,1024]{1,0:T(8,128)(2,1)S(1)}, bf16[96,1024]{1,0:T(8,128)(2,1)S(1)}, u32[]{:S(2)}, u32[]{:S(2)}) %collective-permute-start.5) | collective-permute-done | bytes 196640 | tf_op jit(solution)/shard_map/ppermute | solution.py:394
  29.1 1.3 collective-permute-start.19
  30.4 5.6 %collective-permute-done.6 = bf16[96,1024]{1,0:T(8,128)(2,1)S(1)} collective-permute-done((bf16[96,1024]{1,0:T(8,128)(2,1)S(1)}, bf16[96,1024]{1,0:T(8,128)(2,1)S(1)}, u32[]{:S(2)}, u32[]{:S(2)}) %collective-permute-start.6) | collective-permute-done | bytes 196640 | tf_op jit(solution)/shard_map/ppermute | solution.py:394
  36.0 1.1 collective-permute-done.7
  37.2 0.6 collective-permute-start.10
  37.7 0.8 collective-permute-done.11
  38.9 0.3 collective-permute-start.8
  39.3 1.8 %fusion.19 = f32[384,2048]{1,0:T(8,128)S(1)} fusion(bf16[384,1024]{1,0:T(8,128)(2,1)S(1)} %pad_maximum_fusion.3, bf16[1024,2048]{1,0:T(8,128)(2,1)S(1)} %pad_maximum_fusion), kind=kOutput, calls=%fused_computation.78 | convolution fusion | flops 1610612736 | bytes 8126464 | tf_op jit(solution)/shard_map/dot_general | solution.py:422
  41.1 0.2 fusion.16
  41.4 0.7 collective-permute-start.14
  42.1 7.7 %collective-permute-start.12 = (bf16[192,2048]{1,0:T(8,128)(2,1)S(1)}, bf16[192,2048]{1,0:T(8,128)(2,1)S(1)}, u32[]{:S(2)}, u32[]{:S(2)}) collective-permute-start(bf16[192,2048]{1,0:T(8,128)(2,1)S(1)} %get-tuple-element.90), channel_id=1, source_target_pairs={{0,4},{1,5},{2,6},{3,7},{16,20},{17,21},{18,22},{19,23}} | collective-permute-start | bytes 2359304 | tf_op jit(solution)/shard_map/ppermute | solution.py:445
  49.9 1.8 %fusion.20 = f32[384,2048]{1,0:T(8,128)S(1)} fusion(bf16[384,1024]{1,0:T(8,128)(2,1)S(1)} %pad_maximum_fusion.2, bf16[1024,2048]{1,0:T(8,128)(2,1)S(1)} %pad_maximum_fusion), kind=kOutput, calls=%fused_computation.79 | convolution fusion | flops 1610612736 | bytes 8126464 | tf_op jit(solution)/shard_map/dot_general | solution.py:422
  51.8 0.7 collective-permute-start.20
  52.5 1.3 collective-permute-start.21
  53.8 13.1 %collective-permute-done.12 = bf16[192,2048]{1,0:T(8,128)(2,1)S(1)} collective-permute-done((bf16[192,2048]{1,0:T(8,128)(2,1)S(1)}, bf16[192,2048]{1,0:T(8,128)(2,1)S(1)}, u32[]{:S(2)}, u32[]{:S(2)}) %collective-permute-start.12) | collective-permute-done | bytes 786464 | tf_op jit(solution)/shard_map/ppermute | solution.py:445
  66.9 1.1 add_convert_fusion.3
  68.0 5.5 %collective-permute-start.13 = (bf16[192,2048]{1,0:T(8,128)(2,1)}, bf16[192,2048]{1,0:T(8,128)(2,1)}, u32[]{:S(2)}, u32[]{:S(2)}) collective-permute-start(bf16[192,2048]{1,0:T(8,128)(2,1)} %add_convert_fusion.3), channel_id=1, source_target_pairs={{0,4},{4,8},{1,5},{5,9},{2,6},{6,10},{3,7},{7,11},{16,20},{20,24},... | collective-permute-start | bytes 2359304 | tf_op jit(solution)/shard_map/ppermute | solution.py:445
  73.5 1.8 %add_convert_fusion.2 = (bf16[192,2048]{1,0:T(8,128)(2,1)}, f32[192,2048]{1,0:T(8,128)}) fusion(bf16[192,2048]{1,0:T(8,128)(2,1)S(1)} %collective-permute-done.14, f32[384,2048]{1,0:T(8,128)S(1)} %fusion.20), kind=kLoop, calls=%fused_computation.3 | loop fusion | flops 1179648 | bytes 6291456 | tf_op jit(solution)/shard_map/convert_element_type | solution.py:437
  75.4 0.7 collective-permute-start.22
  76.1 1.3 collective-permute-start.23
  77.4 1.6 collective-permute-start.16
  79.0 1.6 collective-permute-start.1
  81.1 5.9 %take.3 = (f32[48,4,128,128]{3,2,1,0:T(8,128)}, bf16[48,4,128,128]{3,2,1,0:T(8,128)(2,1)}) custom-call(f32[48,4]{1,0:T(8,128)S(1)} %exp.16.last_ref, f32[192,128]{1,0:T(8,128)S(1)} %pad.9.aux_ref, f32[4,4,48,128]{3,2,1,0:T(8,128)S(1)} %get-tuple-element.120.key_ref, f32[4,4,48,128]{3,2,1,0:T(8,128)S(1)} %get-tuple-element.119.value_ref, ...), custom_call_target="tpu_custom_call" | custom-call | flops 67108864 | bytes 8388608 | tf_op jit(solution)/shard_map/take/pallas_call | solution.py:132
  87.0 5.8 %take.4 = (f32[48,4,128,128]{3,2,1,0:T(8,128)}, bf16[48,4,128,128]{3,2,1,0:T(8,128)(2,1)}) custom-call(f32[48,4]{1,0:T(8,128)S(1)} %exp.16.last_ref, f32[192,128]{1,0:T(8,128)S(1)} %pad.9.aux_ref, f32[4,4,48,128]{3,2,1,0:T(8,128)S(1)} %get-tuple-element.120.key_ref, ...), custom_call_target="tpu_custom_call", output_to_operand_aliasing={{0}: (5, {}), {1}: (6, {})} | custom-call | flops 67108864 | bytes 8388608 | tf_op jit(solution)/shard_map/take/pallas_call | solution.py:132
  92.8 6.0 %take.5 = (f32[48,4,128,128]{3,2,1,0:T(8,128)}, bf16[48,4,128,128]{3,2,1,0:T(8,128)(2,1)}) custom-call(f32[48,4]{1,0:T(8,128)S(1)} %exp.16.last_ref, f32[192,128]{1,0:T(8,128)S(1)} %pad.9.aux_ref, f32[4,4,48,128]{3,2,1,0:T(8,128)S(1)} %get-tuple-element.120.key_ref, ...), custom_call_target="tpu_custom_call", output_to_operand_aliasing={{0}: (5, {}), {1}: (6, {})} | custom-call | flops 67108864 | bytes 8388608 | tf_op jit(solution)/shard_map/take/pallas_call | solution.py:132
  98.8 0.7 collective-permute-start.24
  99.6 3.4 %collective-permute-start.27 = (bf16[256,1024]{1,0:T(8,128)(2,1)S(1)}, bf16[256,1024]{1,0:T(8,128)(2,1)S(1)}, u32[]{:S(2)}, u32[]{:S(2)}) collective-permute-start(bf16[256,1024]{1,0:T(8,128)(2,1)S(1)} %copy-done.4), channel_id=1, source_target_pairs={{0,16},{4,20},{8,24},{16,0},{20,4},{24,8},{1,17},{5,21},{9,25},{17... | collective-permute-start | bytes 1572872 | tf_op jit(solution)/shard_map/ppermute | solution.py:371
  103.0 0.7 collective-permute-start.25
  103.7 2.4 %collective-permute-start.28 = (bf16[256,1024]{1,0:T(8,128)(2,1)}, bf16[256,1024]{1,0:T(8,128)(2,1)}, u32[]{:S(2)}, u32[]{:S(2)}) collective-permute-start(bf16[256,1024]{1,0:T(8,128)(2,1)} %collective-permute-done.21.refs_6_), channel_id=1, source_target_pairs={{0,16},{4,20},{16,0},{20,4},{1,17},{5,21},{17,1},{21,5},{2,18},{6,... | collective-permute-start | bytes 1572872 | tf_op jit(solution)/shard_map/ppermute | solution.py:371
  106.2 1.3 add_convert_fusion.1
  107.5 1.5 collective-permute-start.26
  109.0 1.3 add_convert_fusion
  110.3 1.0 fusion.18
  111.3 1.0 fusion.17
  112.3 3.4 %collective-permute-start.29 = (bf16[256,1024]{1,0:T(8,128)(2,1)}, bf16[256,1024]{1,0:T(8,128)(2,1)}, u32[]{:S(2)}, u32[]{:S(2)}) collective-permute-start(bf16[256,1024]{1,0:T(8,128)(2,1)} %collective-permute-done.23.refs_7_), channel_id=1, source_target_pairs={{0,16},{16,0},{1,17},{17,1},{2,18},{18,2},{3,19},{19,3}} | collective-permute-start | bytes 1572872 | tf_op jit(solution)/shard_map/ppermute | solution.py:371
  115.7 0.6 collective-permute-done.27.refs_12_
  116.3 15.6 %collective-permute-start.32 = (bf16[96,2048]{1,0:T(8,128)(2,1)}, bf16[96,2048]{1,0:T(8,128)(2,1)S(1)}, u32[]{:S(2)}, u32[]{:S(2)}) collective-permute-start(bf16[96,2048]{1,0:T(8,128)(2,1)} %get-tuple-element.97), channel_id=1, source_target_pairs={{0,4},{4,8},{8,12},{1,5},{5,9},{9,13},{2,6},{6,10},{10,14},{3,7},{... | collective-permute-start | bytes 1179656 | tf_op jit(solution)/shard_map/ppermute | solution.py:445
  131.9 1.3 collective-permute-start.33
  133.5 7.3 %collective-permute-start.15 = (bf16[96,2048]{1,0:T(8,128)(2,1)}, bf16[96,2048]{1,0:T(8,128)(2,1)S(1)}, u32[]{:S(2)}, u32[]{:S(2)}) collective-permute-start(bf16[96,2048]{1,0:T(8,128)(2,1)} %get-tuple-element.96), channel_id=1, source_target_pairs={{0,4},{4,8},{8,12},{1,5},{5,9},{9,13},{2,6},{6,10},{10,14},{3,7},{... | collective-permute-start | bytes 1179656 | tf_op jit(solution)/shard_map/ppermute | solution.py:445
  140.8 1.5 collective-permute-start.17
  142.4 6.5 %finish.3 = (bf16[96,2048]{1,0:T(8,128)(2,1)S(1)}, bf16[96,2048]{1,0:T(8,128)(2,1)S(1)}) custom-call(s32[8]{0:T(128)S(1)} %pad_add_fusion.position_ref, f32[192,128]{1,0:T(8,128)S(1)} %pad.8.aux_ref, f32[1,128]{1,0:T(1,128)S(1)} %bitcast.29, f32[192,2048]{1,0:T(8,128)} %get-tuple-element.89.own_ref, bf16[96,2048]{1,0:T(8,128)(2,1)S(1)} %collective-permute-done.32.right_ref, ...), custom_call_target="tpu_custom_call" | custom-call | flops 100663296 | bytes 3145728 | tf_op jit(solution)/shard_map/finish/pallas_call | solution.py:261
  149.0 4.9 %collective-permute-done.17.left_ref = bf16[96,2048]{1,0:T(8,128)(2,1)S(1)} collective-permute-done((bf16[96,2048]{1,0:T(8,128)(2,1)}, bf16[96,2048]{1,0:T(8,128)(2,1)S(1)}, u32[]{:S(2)}, u32[]{:S(2)}) %collective-permute-start.17) | collective-permute-done | bytes 393248 | tf_op jit(solution)/shard_map/ppermute | solution.py:445
  153.8 6.5 %finish.2 = (bf16[96,2048]{1,0:T(8,128)(2,1)S(1)}, bf16[96,2048]{1,0:T(8,128)(2,1)S(1)}) custom-call(s32[8]{0:T(128)S(1)} %pad_add_fusion.position_ref, f32[192,128]{1,0:T(8,128)S(1)} %pad.8.aux_ref, f32[1,128]{1,0:T(1,128)S(1)} %bitcast.30, f32[192,2048]{1,0:T(8,128)} %get-tuple-element.89.own_ref, bf16[96,2048]{1,0:T(8,128)(2,1)S(1)} %collective-permute-done.15.right_ref, ...), custom_call_target="tpu_custom_call" | custom-call | flops 100663296 | bytes 3145728 | tf_op jit(solution)/shard_map/finish/pallas_call | solution.py:261
  160.5 0.6 collective-permute-start.35
  161.1 1.0 collective-permute-done.30
  162.2 0.6 collective-permute-start.31
  162.8 5.5 %collective-permute-done.35 = bf16[96,1024]{1,0:T(8,128)(2,1)S(1)} collective-permute-done((bf16[96,1024]{1,0:T(8,128)(2,1)S(1)}, bf16[96,1024]{1,0:T(8,128)(2,1)S(1)}, u32[]{:S(2)}, u32[]{:S(2)}) %collective-permute-start.35) | collective-permute-done | bytes 196640 | tf_op jit(solution)/shard_map/ppermute | solution.py:334
  168.4 3.7 %collective-permute-done.31 = bf16[96,1024]{1,0:T(8,128)(2,1)S(1)} collective-permute-done((bf16[96,1024]{1,0:T(8,128)(2,1)S(1)}, bf16[96,1024]{1,0:T(8,128)(2,1)S(1)}, u32[]{:S(2)}, u32[]{:S(2)}) %collective-permute-start.31) | collective-permute-done | bytes 196640 | tf_op jit(solution)/shard_map/ppermute | solution.py:334
  172.1 0.8 pad_maximum_fusion.4
  (98 shorter events, 2.1 us)
Async XLA Ops:
  0.6 7.2 %copy-start.8 = (bf16[512,1024]{1,0:T(8,128)(2,1)S(1)}, bf16[512,1024]{1,0:T(8,128)(2,1)}, u32[]{:S(2)}) copy-start(bf16[512,1024]{1,0:T(8,128)(2,1)} %param.32) | copy-start | bytes 3145732
  2.6 11.2 %copy-start.9 = (bf16[1024,512]{1,0:T(8,128)(2,1)S(1)}, bf16[1024,512]{1,0:T(8,128)(2,1)}, u32[]{:S(2)}) copy-start(bf16[1024,512]{1,0:T(8,128)(2,1)} %param.25) | copy-start | bytes 3145732
  3.7 75.2 %collective-permute-start = (f32[192,33]{0,1:T(8,128)S(1)}, f32[192,33]{0,1:T(8,128)S(1)}, u32[]{:S(2)}, u32[]{:S(2)}) collective-permute-start(f32[192,33]{0,1:T(8,128)S(1)} %pad_maximum_fusion.5), channel_id=1, source_target_pairs={{0,1},{1,0},{2,3},{3,2},{4,5},{5,4},{6,7},{7,6},{8,9},{9,8},{10,11... | collective-permute-start | bytes 76040 | tf_op jit(solution)/shard_map/ppermute | solution.py:334
  5.1 10.9 %collective-permute-start.4 = (bf16[96,1024]{1,0:T(8,128)(2,1)}, bf16[96,1024]{1,0:T(8,128)(2,1)}, u32[]{:S(2)}, u32[]{:S(2)}) collective-permute-start(bf16[96,1024]{1,0:T(8,128)(2,1)} %get-tuple-element.111), channel_id=1, source_target_pairs={{0,3},{1,2},{2,1},{3,0},{4,7},{5,6},{6,5},{7,4},{8,11},{9,10},{10,... | collective-permute-start | bytes 589832 | tf_op jit(solution)/shard_map/ppermute | solution.py:334
  7.7 10.0 %collective-permute-start.3 = (bf16[96,1024]{1,0:T(8,128)(2,1)}, bf16[96,1024]{1,0:T(8,128)(2,1)}, u32[]{:S(2)}, u32[]{:S(2)}) collective-permute-start(bf16[96,1024]{1,0:T(8,128)(2,1)} %get-tuple-element.112), channel_id=1, source_target_pairs={{0,2},{1,3},{2,0},{3,1},{4,6},{5,7},{6,4},{7,5},{8,10},{9,11},{10,... | collective-permute-start | bytes 589832 | tf_op jit(solution)/shard_map/ppermute | solution.py:334
  7.7 10.0 %collective-permute-start.2 = (bf16[96,1024]{1,0:T(8,128)(2,1)}, bf16[96,1024]{1,0:T(8,128)(2,1)}, u32[]{:S(2)}, u32[]{:S(2)}) collective-permute-start(bf16[96,1024]{1,0:T(8,128)(2,1)} %get-tuple-element.113), channel_id=1, source_target_pairs={{0,1},{1,0},{2,3},{3,2},{4,5},{5,4},{6,7},{7,6},{8,9},{9,8},{10,11... | collective-permute-start | bytes 589832 | tf_op jit(solution)/shard_map/ppermute | solution.py:334
  8.7 43.0 %collective-permute-start.18 = (bf16[256,1024]{1,0:T(8,128)(2,1)S(1)}, bf16[256,1024]{1,0:T(8,128)(2,1)S(1)}, u32[]{:S(2)}, u32[]{:S(2)}) collective-permute-start(bf16[256,1024]{1,0:T(8,128)(2,1)S(1)} %get-tuple-element.70.refs_1_), channel_id=1, source_target_pairs={{0,4},{4,8},{8,12},{1,5},{5,9},{9,13},{2,6},{6,10},{10,14},{3,7},{... | collective-permute-start | bytes 1572872 | tf_op jit(solution)/shard_map/ppermute | solution.py:360
  13.8 2.2 %copy-start.15 = (s32[48]{0:T(128)S(1)}, s32[48]{0:T(128)}, u32[]{:S(2)}) copy-start(s32[48]{0:T(128)} %param.38) | copy-start | bytes 580
  16.0 8.8 %copy-start.10 = (f32[48,4,4]{0,2,1:T(4,128)S(1)}, f32[48,4,4]{0,2,1:T(4,128)}, u32[]{:S(2)}) copy-start(f32[48,4,4]{0,2,1:T(4,128)} %param.37) | copy-start | bytes 9220
  16.0 8.8 %copy-start.11 = (f32[48,4,4]{0,2,1:T(4,128)S(1)}, f32[48,4,4]{0,2,1:T(4,128)}, u32[]{:S(2)}) copy-start(f32[48,4,4]{0,2,1:T(4,128)} %param.36) | copy-start | bytes 9220
  16.0 21.1 %copy-start.14 = (s32[7]{0:T(128)S(1)}, s32[7]{0:T(128)}, u32[]{:S(2)}) copy-start(s32[7]{0:T(128)} %constant.185.clone) | copy-start | bytes 88
  19.0 10.1 %collective-permute-start.5 = (bf16[96,1024]{1,0:T(8,128)(2,1)S(1)}, bf16[96,1024]{1,0:T(8,128)(2,1)S(1)}, u32[]{:S(2)}, u32[]{:S(2)}) collective-permute-start(bf16[96,1024]{1,0:T(8,128)(2,1)S(1)} %get-tuple-element.45), channel_id=1, source_target_pairs={{0,4},{4,8},{8,12},{12,0},{1,5},{5,9},{9,13},{13,1},{2,6},{6,10},{... | collective-permute-start | bytes 589832 | tf_op jit(solution)/shard_map/ppermute | solution.py:394
  20.9 15.2 %collective-permute-start.6 = (bf16[96,1024]{1,0:T(8,128)(2,1)S(1)}, bf16[96,1024]{1,0:T(8,128)(2,1)S(1)}, u32[]{:S(2)}, u32[]{:S(2)}) collective-permute-start(bf16[96,1024]{1,0:T(8,128)(2,1)S(1)} %get-tuple-element.46), channel_id=1, source_target_pairs={{0,8},{4,12},{8,0},{12,4},{1,9},{5,13},{9,1},{13,5},{2,10},{6,14},... | collective-permute-start | bytes 589832 | tf_op jit(solution)/shard_map/ppermute | solution.py:394
  23.4 13.7 %collective-permute-start.7 = (bf16[96,1024]{1,0:T(8,128)(2,1)S(1)}, bf16[96,1024]{1,0:T(8,128)(2,1)S(1)}, u32[]{:S(2)}, u32[]{:S(2)}) collective-permute-start(bf16[96,1024]{1,0:T(8,128)(2,1)S(1)} %get-tuple-element.47), channel_id=1, source_target_pairs={{0,12},{4,0},{8,4},{12,8},{1,13},{5,1},{9,5},{13,9},{2,14},{6,2},{... | collective-permute-start | bytes 589832 | tf_op jit(solution)/shard_map/ppermute | solution.py:394
  29.1 22.6 %collective-permute-start.19 = (bf16[256,1024]{1,0:T(8,128)(2,1)S(1)}, bf16[256,1024]{1,0:T(8,128)(2,1)S(1)}, u32[]{:S(2)}, u32[]{:S(2)}) collective-permute-start(bf16[256,1024]{1,0:T(8,128)(2,1)S(1)} %get-tuple-element.70.refs_1_), channel_id=1, source_target_pairs={{4,0},{8,4},{12,8},{5,1},{9,5},{13,9},{6,2},{10,6},{14,10},{7,3},{... | collective-permute-start | bytes 1572872 | tf_op jit(solution)/shard_map/ppermute | solution.py:362
  37.1 1.4 collective-permute-start.11
  37.2 1.7 collective-permute-start.10
  38.6 2.8 %collective-permute-start.9 = (bf16[96,1024]{1,0:T(8,128)(2,1)S(1)}, bf16[96,1024]{1,0:T(8,128)(2,1)S(1)}, u32[]{:S(2)}, u32[]{:S(2)}) collective-permute-start(bf16[96,1024]{1,0:T(8,128)(2,1)S(1)} %collective-permute-done.6), channel_id=1, source_target_pairs={{0,1},{1,0},{2,3},{3,2},{4,5},{5,4},{6,7},{7,6},{8,9},{9,8},{10,11... | collective-permute-start | bytes 589832 | tf_op jit(solution)/shard_map/ppermute | solution.py:334
  38.9 3.3 %collective-permute-start.8 = (bf16[96,1024]{1,0:T(8,128)(2,1)S(1)}, bf16[96,1024]{1,0:T(8,128)(2,1)S(1)}, u32[]{:S(2)}, u32[]{:S(2)}) collective-permute-start(bf16[96,1024]{1,0:T(8,128)(2,1)S(1)} %get-tuple-element.48), channel_id=1, source_target_pairs={{0,1},{1,0},{2,3},{3,2},{4,5},{5,4},{6,7},{7,6},{8,9},{9,8},{10,11... | collective-permute-start | bytes 589832 | tf_op jit(solution)/shard_map/ppermute | solution.py:334
  41.1 8.8 %copy-start.1 = (f32[384,2048]{1,0:T(8,128)}, f32[384,2048]{1,0:T(8,128)S(1)}, u32[]{:S(2)}) copy-start(f32[384,2048]{1,0:T(8,128)S(1)} %fusion.19) | copy-start | bytes 9437188
  41.4 32.1 %collective-permute-start.14 = (bf16[192,2048]{1,0:T(8,128)(2,1)S(1)}, bf16[192,2048]{1,0:T(8,128)(2,1)S(1)}, u32[]{:S(2)}, u32[]{:S(2)}) collective-permute-start(bf16[192,2048]{1,0:T(8,128)(2,1)S(1)} %get-tuple-element.91), channel_id=1, source_target_pairs={{12,8},{13,9},{14,10},{15,11},{28,24},{29,25},{30,26},{31,27}} | collective-permute-start | bytes 2359304 | tf_op jit(solution)/shard_map/ppermute | solution.py:445
  42.1 24.8 %collective-permute-start.12 = (bf16[192,2048]{1,0:T(8,128)(2,1)S(1)}, bf16[192,2048]{1,0:T(8,128)(2,1)S(1)}, u32[]{:S(2)}, u32[]{:S(2)}) collective-permute-start(bf16[192,2048]{1,0:T(8,128)(2,1)S(1)} %get-tuple-element.90), channel_id=1, source_target_pairs={{0,4},{1,5},{2,6},{3,7},{16,20},{17,21},{18,22},{19,23}} | collective-permute-start | bytes 2359304 | tf_op jit(solution)/shard_map/ppermute | solution.py:445
  51.8 23.6 %copy-start.3 = (bf16[256,1024]{1,0:T(8,128)(2,1)}, bf16[256,1024]{1,0:T(8,128)(2,1)S(1)}, u32[]{:S(2)}) copy-start(bf16[256,1024]{1,0:T(8,128)(2,1)S(1)} %collective-permute-done.19.refs_5_) | copy-start | bytes 1572868
  51.8 23.6 %collective-permute-start.20 = (bf16[256,1024]{1,0:T(8,128)(2,1)S(1)}, bf16[256,1024]{1,0:T(8,128)(2,1)S(1)}, u32[]{:S(2)}, u32[]{:S(2)}) collective-permute-start(bf16[256,1024]{1,0:T(8,128)(2,1)S(1)} %collective-permute-done.18.refs_2_), channel_id=1, source_target_pairs={{4,8},{8,12},{5,9},{9,13},{6,10},{10,14},{7,11},{11,15},{20,24},{2... | collective-permute-start | bytes 1572872 | tf_op jit(solution)/shard_map/ppermute | solution.py:360
  52.5 22.9 %collective-permute-start.21 = (bf16[256,1024]{1,0:T(8,128)(2,1)S(1)}, bf16[256,1024]{1,0:T(8,128)(2,1)}, u32[]{:S(2)}, u32[]{:S(2)}) collective-permute-start(bf16[256,1024]{1,0:T(8,128)(2,1)S(1)} %collective-permute-done.19.refs_5_), channel_id=1, source_target_pairs={{4,0},{8,4},{5,1},{9,5},{6,2},{10,6},{7,3},{11,7},{20,16},{24,20},... | collective-permute-start | bytes 1572872 | tf_op jit(solution)/shard_map/ppermute | solution.py:362
  68.0 9.3 %copy-start.16 = (f32[4]{0:T(128)S(1)}, f32[4]{0:T(128)}, u32[]{:S(2)}) copy-start(f32[4]{0:T(128)} %param.28) | copy-start | bytes 52
  68.0 12.6 %copy-start.12 = (f32[48,4,4]{0,2,1:T(4,128)S(1)}, f32[48,4,4]{0,2,1:T(4,128)}, u32[]{:S(2)}) copy-start(f32[48,4,4]{0,2,1:T(4,128)} %param.30) | copy-start | bytes 9220
  68.0 35.7 %collective-permute-start.13 = (bf16[192,2048]{1,0:T(8,128)(2,1)}, bf16[192,2048]{1,0:T(8,128)(2,1)}, u32[]{:S(2)}, u32[]{:S(2)}) collective-permute-start(bf16[192,2048]{1,0:T(8,128)(2,1)} %add_convert_fusion.3), channel_id=1, source_target_pairs={{0,4},{4,8},{1,5},{5,9},{2,6},{6,10},{3,7},{7,11},{16,20},{20,24},... | collective-permute-start | bytes 2359304 | tf_op jit(solution)/shard_map/ppermute | solution.py:445
  75.4 24.2 %collective-permute-start.22 = (bf16[256,1024]{1,0:T(8,128)(2,1)S(1)}, bf16[256,1024]{1,0:T(8,128)(2,1)S(1)}, u32[]{:S(2)}, u32[]{:S(2)}) collective-permute-start(bf16[256,1024]{1,0:T(8,128)(2,1)S(1)} %collective-permute-done.20.refs_3_), channel_id=1, source_target_pairs={{8,12},{9,13},{10,14},{11,15},{24,28},{25,29},{26,30},{27,31}} | collective-permute-start | bytes 1572872 | tf_op jit(solution)/shard_map/ppermute | solution.py:360
  76.1 26.9 %collective-permute-start.23 = (bf16[256,1024]{1,0:T(8,128)(2,1)}, bf16[256,1024]{1,0:T(8,128)(2,1)}, u32[]{:S(2)}, u32[]{:S(2)}) collective-permute-start(bf16[256,1024]{1,0:T(8,128)(2,1)} %collective-permute-done.21.refs_6_), channel_id=1, source_target_pairs={{4,0},{5,1},{6,2},{7,3},{20,16},{21,17},{22,18},{23,19}} | collective-permute-start | bytes 1572872 | tf_op jit(solution)/shard_map/ppermute | solution.py:362
  77.4 30.1 %collective-permute-start.16 = (bf16[192,2048]{1,0:T(8,128)(2,1)}, bf16[192,2048]{1,0:T(8,128)(2,1)}, u32[]{:S(2)}, u32[]{:S(2)}) collective-permute-start(bf16[192,2048]{1,0:T(8,128)(2,1)} %get-tuple-element.88), channel_id=1, source_target_pairs={{8,4},{12,8},{9,5},{13,9},{10,6},{14,10},{11,7},{15,11},{24,20},{2... | collective-permute-start | bytes 2359304 | tf_op jit(solution)/shard_map/ppermute | solution.py:445
  79.0 19.9 %collective-permute-start.1 = (f32[192,33]{0,1:T(8,128)S(1)}, f32[192,33]{0,1:T(8,128)S(1)}, u32[]{:S(2)}, u32[]{:S(2)}) collective-permute-start(f32[192,33]{0,1:T(8,128)S(1)} %fusion.14), channel_id=1, source_target_pairs={{0,2},{1,3},{2,0},{3,1},{4,6},{5,7},{6,4},{7,5},{8,10},{9,11},{10,... | collective-permute-start | bytes 76040 | tf_op jit(solution)/shard_map/ppermute | solution.py:334
  92.8 6.8 %copy-start.4 = (bf16[256,1024]{1,0:T(8,128)(2,1)S(1)}, bf16[256,1024]{1,0:T(8,128)(2,1)}, u32[]{:S(2)}) copy-start(bf16[256,1024]{1,0:T(8,128)(2,1)} %copy-done.3) | copy-start | bytes 1572868
  92.8 13.4 %copy-start.2 = (f32[384,2048]{1,0:T(8,128)S(1)}, f32[384,2048]{1,0:T(8,128)}, u32[]{:S(2)}) copy-start(f32[384,2048]{1,0:T(8,128)} %copy-done.1) | copy-start | bytes 9437188
  98.8 13.4 %collective-permute-start.24 = (bf16[256,1024]{1,0:T(8,128)(2,1)S(1)}, bf16[256,1024]{1,0:T(8,128)(2,1)S(1)}, u32[]{:S(2)}, u32[]{:S(2)}) collective-permute-start(bf16[256,1024]{1,0:T(8,128)(2,1)S(1)} %collective-permute-done.18.refs_2_), channel_id=1, source_target_pairs={{4,20},{8,24},{12,28},{20,4},{24,8},{28,12},{5,21},{9,25},{13,29},... | collective-permute-start | bytes 1572872 | tf_op jit(solution)/shard_map/ppermute | solution.py:370
  99.6 16.7 %collective-permute-start.27 = (bf16[256,1024]{1,0:T(8,128)(2,1)S(1)}, bf16[256,1024]{1,0:T(8,128)(2,1)S(1)}, u32[]{:S(2)}, u32[]{:S(2)}) collective-permute-start(bf16[256,1024]{1,0:T(8,128)(2,1)S(1)} %copy-done.4), channel_id=1, source_target_pairs={{0,16},{4,20},{8,24},{16,0},{20,4},{24,8},{1,17},{5,21},{9,25},{17... | collective-permute-start | bytes 1572872 | tf_op jit(solution)/shard_map/ppermute | solution.py:371
  103.0 28.8 %collective-permute-start.25 = (bf16[256,1024]{1,0:T(8,128)(2,1)S(1)}, bf16[256,1024]{1,0:T(8,128)(2,1)S(1)}, u32[]{:S(2)}, u32[]{:S(2)}) collective-permute-start(bf16[256,1024]{1,0:T(8,128)(2,1)S(1)} %collective-permute-done.20.refs_3_), channel_id=1, source_target_pairs={{8,24},{12,28},{24,8},{28,12},{9,25},{13,29},{25,9},{29,13},{10,26... | collective-permute-start | bytes 1572872 | tf_op jit(solution)/shard_map/ppermute | solution.py:370
  103.7 29.7 %collective-permute-start.28 = (bf16[256,1024]{1,0:T(8,128)(2,1)}, bf16[256,1024]{1,0:T(8,128)(2,1)}, u32[]{:S(2)}, u32[]{:S(2)}) collective-permute-start(bf16[256,1024]{1,0:T(8,128)(2,1)} %collective-permute-done.21.refs_6_), channel_id=1, source_target_pairs={{0,16},{4,20},{16,0},{20,4},{1,17},{5,21},{17,1},{21,5},{2,18},{6,... | collective-permute-start | bytes 1572872 | tf_op jit(solution)/shard_map/ppermute | solution.py:371
  107.5 25.7 %copy-start.13 = (f32[4]{0:T(128)S(1)}, f32[4]{0:T(128)}, u32[]{:S(2)}) copy-start(f32[4]{0:T(128)} %param.29) | copy-start | bytes 52
  107.5 34.9 %copy-start = (f32[128]{0:T(128)S(1)}, f32[128]{0:T(128)}, u32[]{:S(2)}) copy-start(f32[128]{0:T(128)} %param.31) | copy-start | bytes 1540
  107.5 33.3 %collective-permute-start.26 = (bf16[256,1024]{1,0:T(8,128)(2,1)S(1)}, bf16[256,1024]{1,0:T(8,128)(2,1)}, u32[]{:S(2)}, u32[]{:S(2)}) collective-permute-start(bf16[256,1024]{1,0:T(8,128)(2,1)S(1)} %collective-permute-done.22.refs_4_), channel_id=1, source_target_pairs={{12,28},{28,12},{13,29},{29,13},{14,30},{30,14},{15,31},{31,15}} | collective-permute-start | bytes 1572872 | tf_op jit(solution)/shard_map/ppermute | solution.py:370
  112.3 19.6 %copy-start.5 = (bf16[256,1024]{1,0:T(8,128)(2,1)}, bf16[256,1024]{1,0:T(8,128)(2,1)S(1)}, u32[]{:S(2)}) copy-start(bf16[256,1024]{1,0:T(8,128)(2,1)S(1)} %collective-permute-done.24.refs_9_) | copy-start | bytes 1572868
  112.3 30.0 %collective-permute-start.29 = (bf16[256,1024]{1,0:T(8,128)(2,1)}, bf16[256,1024]{1,0:T(8,128)(2,1)}, u32[]{:S(2)}, u32[]{:S(2)}) collective-permute-start(bf16[256,1024]{1,0:T(8,128)(2,1)} %collective-permute-done.23.refs_7_), channel_id=1, source_target_pairs={{0,16},{16,0},{1,17},{17,1},{2,18},{18,2},{3,19},{19,3}} | collective-permute-start | bytes 1572872 | tf_op jit(solution)/shard_map/ppermute | solution.py:371
  116.3 16.9 %copy-start.6 = (bf16[256,1024]{1,0:T(8,128)(2,1)}, bf16[256,1024]{1,0:T(8,128)(2,1)S(1)}, u32[]{:S(2)}) copy-start(bf16[256,1024]{1,0:T(8,128)(2,1)S(1)} %collective-permute-done.27.refs_12_) | copy-start | bytes 1572868
  116.3 26.1 %collective-permute-start.32 = (bf16[96,2048]{1,0:T(8,128)(2,1)}, bf16[96,2048]{1,0:T(8,128)(2,1)S(1)}, u32[]{:S(2)}, u32[]{:S(2)}) collective-permute-start(bf16[96,2048]{1,0:T(8,128)(2,1)} %get-tuple-element.97), channel_id=1, source_target_pairs={{0,4},{4,8},{8,12},{1,5},{5,9},{9,13},{2,6},{6,10},{10,14},{3,7},{... | collective-permute-start | bytes 1179656 | tf_op jit(solution)/shard_map/ppermute | solution.py:445
  131.9 1.3 copy-start.7
  131.9 10.5 %collective-permute-start.33 = (bf16[96,2048]{1,0:T(8,128)(2,1)}, bf16[96,2048]{1,0:T(8,128)(2,1)S(1)}, u32[]{:S(2)}, u32[]{:S(2)}) collective-permute-start(bf16[96,2048]{1,0:T(8,128)(2,1)} %get-tuple-element.95), channel_id=1, source_target_pairs={{4,0},{8,4},{12,8},{5,1},{9,5},{13,9},{6,2},{10,6},{14,10},{7,3},{... | collective-permute-start | bytes 1179656 | tf_op jit(solution)/shard_map/ppermute | solution.py:445
  133.5 15.5 %collective-permute-start.15 = (bf16[96,2048]{1,0:T(8,128)(2,1)}, bf16[96,2048]{1,0:T(8,128)(2,1)S(1)}, u32[]{:S(2)}, u32[]{:S(2)}) collective-permute-start(bf16[96,2048]{1,0:T(8,128)(2,1)} %get-tuple-element.96), channel_id=1, source_target_pairs={{0,4},{4,8},{8,12},{1,5},{5,9},{9,13},{2,6},{6,10},{10,14},{3,7},{... | collective-permute-start | bytes 1179656 | tf_op jit(solution)/shard_map/ppermute | solution.py:445
  140.8 13.0 %collective-permute-start.17 = (bf16[96,2048]{1,0:T(8,128)(2,1)}, bf16[96,2048]{1,0:T(8,128)(2,1)S(1)}, u32[]{:S(2)}, u32[]{:S(2)}) collective-permute-start(bf16[96,2048]{1,0:T(8,128)(2,1)} %get-tuple-element.94), channel_id=1, source_target_pairs={{4,0},{8,4},{12,8},{5,1},{9,5},{13,9},{6,2},{10,6},{14,10},{7,3},{... | collective-permute-start | bytes 1179656 | tf_op jit(solution)/shard_map/ppermute | solution.py:445
  148.9 11.5 %collective-permute-start.34 = (bf16[96,2048]{1,0:T(8,128)(2,1)S(1)}, bf16[96,2048]{1,0:T(8,128)(2,1)S(1)}, u32[]{:S(2)}, u32[]{:S(2)}) collective-permute-start(bf16[96,2048]{1,0:T(8,128)(2,1)S(1)} %get-tuple-element.84), channel_id=1, source_target_pairs={{0,1},{1,0},{2,3},{3,2},{4,5},{5,4},{6,7},{7,6},{8,9},{9,8},{10,11... | collective-permute-start | bytes 1179656 | tf_op jit(solution)/shard_map/ppermute | solution.py:334
  160.3 1.8 %collective-permute-start.30 = (bf16[96,2048]{1,0:T(8,128)(2,1)S(1)}, bf16[96,2048]{1,0:T(8,128)(2,1)S(1)}, u32[]{:S(2)}, u32[]{:S(2)}) collective-permute-start(bf16[96,2048]{1,0:T(8,128)(2,1)S(1)} %get-tuple-element.82), channel_id=1, source_target_pairs={{0,1},{1,0},{2,3},{3,2},{4,5},{5,4},{6,7},{7,6},{8,9},{9,8},{10,11... | collective-permute-start | bytes 1179656 | tf_op jit(solution)/shard_map/ppermute | solution.py:334
  160.5 7.8 %collective-permute-start.35 = (bf16[96,1024]{1,0:T(8,128)(2,1)S(1)}, bf16[96,1024]{1,0:T(8,128)(2,1)S(1)}, u32[]{:S(2)}, u32[]{:S(2)}) collective-permute-start(bf16[96,1024]{1,0:T(8,128)(2,1)S(1)} %slice.88), channel_id=1, source_target_pairs={{0,2},{1,3},{2,0},{3,1},{4,6},{5,7},{6,4},{7,5},{8,10},{9,11},{10,... | collective-permute-start | bytes 589832 | tf_op jit(solution)/shard_map/ppermute | solution.py:334
  162.2 9.9 %collective-permute-start.31 = (bf16[96,1024]{1,0:T(8,128)(2,1)S(1)}, bf16[96,1024]{1,0:T(8,128)(2,1)S(1)}, u32[]{:S(2)}, u32[]{:S(2)}) collective-permute-start(bf16[96,1024]{1,0:T(8,128)(2,1)S(1)} %slice.89), channel_id=1, source_target_pairs={{0,2},{1,3},{2,0},{3,1},{4,6},{5,7},{6,4},{7,5},{8,10},{9,11},{10,... | collective-permute-start | bytes 589832 | tf_op jit(solution)/shard_map/ppermute | solution.py:334
